TPU v7x, 512 devices: a whole 4x4x16 slice. The times are simulated.
512 devices in a mesh: ep: 32 (over z, core), tp: 16 (over y, x).
Axes of the slice: x: 4, y: 4, z: 16, core: 2. Of those that a mesh axis runs over, the one named last changes fastest.
Arguments:
- tokens: bfloat16 [512, 2048], P('ep'), may hold values from -6 to 6
- attn_gain: bfloat16 [2048], replicated, may hold values from 0.099609375 to 1.8984375
- w_query: bfloat16 [2048, 1024], P('ep', 'tp'), may hold values from -0.125 to 0.125
- w_key: bfloat16 [2048, 1024], P('ep', 'tp'), may hold values from -0.125 to 0.125
- w_value: bfloat16 [2048, 1024], P('ep', 'tp'), may hold values from -0.125 to 0.125
- w_forget: bfloat16 [2048, 16], P('ep', 'tp'), may hold values from -0.375 to 0.375
- forget_bias: float32 [16], P('tp'), may hold values from -2 to 2
- cache_keys: bfloat16 [512, 16, 1024, 64], P('ep', 'tp'), may hold values from -200 to 200
- cache_values: bfloat16 [512, 16, 1024, 64], P('ep', 'tp'), may hold values from -6 to 6
- cache_gates: float32 [512, 16, 1024], P('ep', 'tp'), may hold values from -256 to 0, as said below
- lengths: int32 [512], P('ep'), may hold values from 1 to 1024, 262144 in all
- w_out: bfloat16 [1024, 2048], P('tp', 'ep'), may hold values from -0.1875 to 0.1875
- moe_gain: bfloat16 [2048], replicated, may hold values from 0.099609375 to 1.8984375
- routing: int32 [512, 4], P('ep'), may hold values from 0 to 31, all different within a row; in each aligned block of 16 rows (0 to 15, 16 to 31, ...) at most 4 rows name the same one
- route_weight: float32 [512, 4], P('ep'), may hold values from 0.1 to 1
- w_gate: bfloat16 [32, 2048, 1024], P('ep', None, 'tp')
- w_up: bfloat16 [32, 2048, 1024], P('ep', None, 'tp')
- w_down: bfloat16 [32, 1024, 2048], P('ep', 'tp'), may hold values from -0.1875 to 0.1875
Outputs:
- layer_out: bfloat16 [512, 2048], P('ep')
Inputs may be any that keep to these rules, and one draw needn't show every extreme that they name: `routing`: within the rows of one device (aligned blocks of 16 rows) no expert is named more than 4 times, a bound that some block reaches; each row names 4 different experts. lengths[s] is at least 1 and at most 1024; some sequence has exactly 1024. cache_gates[s, h, p] is the sum of the log forget gates of positions 0 to p of sequence s in head h; it never rises along p.
All inputs are finite; a program needn't handle non-finite values. No bound on the sum of `lengths` on one device may be relied on, other than what follows from the above.
Results may differ from a plain program's by a relative error of at most 0.012.
The roundings to bfloat16 on the way count: a program that leaves them out, or rounds other values in their place, can miss the bound.
Values may be sent and summed in bfloat16 or wider, within the bound.
No kernel may reach another device: no remote copies, remote signals or barrier semaphores. Data moves between devices by JAX's collectives and lax.ppermute only.
A program may use at most 64 MiB of HBM per device.

v0:
```python
import jax
import jax.numpy as jnp
from jax import lax
from jax.sharding import PartitionSpec as P

NORM_EPSILON = 1e-06
CLAMP_LIMIT = 7.0
SIGMOID_SLOPE = 1.702


def sent_together(arrays, axis, dim, along):
    widths = [a.shape[along] for a in arrays]
    both = jnp.concatenate(arrays, axis=along)
    result = lax.all_gather(both, axis, axis=dim, tiled=True)
    return tuple(jnp.split(result, [sum(widths[:k]) for k in range(1, len(widths))], axis=along))


def from_everyone(shard, axis):
    size = lax.axis_size(axis)
    return lax.all_to_all(
        jnp.broadcast_to(shard[None], (size, *shard.shape)), axis, 0, 0, tiled=True
    )


def laid_out(tiles, dim):
    shape = list(tiles.shape[1:])
    shape[dim] *= tiles.shape[0]
    return jnp.moveaxis(tiles, 0, dim).reshape(shape)


def gathered_copies(shard, axis, dim):
    tiles = from_everyone(shard, axis)
    return laid_out(tiles, dim)


def taken_together(shard, axis):
    everything = from_everyone(shard, axis)
    return jnp.sum(everything, axis=0)


def split_up(shard, dim, size):
    shape = shard.shape
    tiles = shard.reshape(*shape[:dim], size, shape[dim] // size, *shape[dim + 1 :])
    return jnp.moveaxis(tiles, dim, 0)


def sum_at_owner(shard, axis, dim):
    size = lax.axis_size(axis)
    tiles = lax.all_to_all(split_up(shard, dim, size), axis, 0, 0, tiled=True)
    return jnp.sum(tiles, axis=0)


def rms_norm(values, gain_vector):
    widened = values.astype(jnp.float32)
    scaled = widened * lax.rsqrt(jnp.mean(widened * widened, axis=-1, keepdims=True) + NORM_EPSILON)
    return (scaled * gain_vector.astype(jnp.float32)).astype(jnp.bfloat16)


def hidden_units(token_rows, gate_matrix, up_matrix):
    gate_pre = jnp.dot(token_rows, gate_matrix, preferred_element_type=jnp.float32)
    up_pre = jnp.dot(token_rows, up_matrix, preferred_element_type=jnp.float32)
    gate_cut = jnp.minimum(gate_pre, CLAMP_LIMIT)
    up_cut = jnp.clip(up_pre, -CLAMP_LIMIT, CLAMP_LIMIT)
    return ((up_cut + 1.0) * gate_cut * jax.nn.sigmoid(SIGMOID_SLOPE * gate_cut)).astype(
        jnp.bfloat16
    )


def expert_partial(token_rows, gate_matrix, up_matrix, down_matrix):
    hidden = hidden_units(token_rows, gate_matrix, up_matrix)
    return jnp.dot(hidden, down_matrix, preferred_element_type=jnp.float32)


def local(
    tokens,
    attn_gain,
    w_query,
    w_key,
    w_value,
    w_forget,
    forget_bias,
    cache_keys,
    cache_values,
    cache_gates,
    lengths,
    w_out,
    moe_gain,
    routing,
    route_weight,
    w_gate,
    w_up,
    w_down,
):
    seq_count, model_width = tokens.shape
    heads_here = forget_bias.shape[0]
    head_size = cache_keys.shape[3]
    inner = heads_here * head_size
    gate_matrix, up_matrix, down_matrix = (w_gate[0], w_up[0], w_down[0])
    normed = rms_norm(tokens, attn_gain)
    projected = jnp.dot(
        normed,
        jnp.concatenate(sent_together((w_query, w_key, w_value, w_forget), "ep", 0, 1), axis=1),
        preferred_element_type=jnp.float32,
    )
    query = projected[:, :inner].astype(jnp.bfloat16).reshape(seq_count, heads_here, head_size)
    key_new = (
        projected[:, inner : 2 * inner]
        .astype(jnp.bfloat16)
        .reshape(seq_count, heads_here, head_size)
    )
    value_new = (
        projected[:, 2 * inner : 3 * inner]
        .astype(jnp.bfloat16)
        .reshape(seq_count, heads_here, head_size)
    )
    log_gate = jax.nn.log_sigmoid(projected[:, 3 * inner :] + forget_bias)
    scale = head_size ** (-0.5)
    positions = jnp.arange(cache_keys.shape[2], dtype=jnp.int32)
    valid = positions[None, None, :] < lengths[:, None, None]
    is_last = positions[None, None, :] == lengths[:, None, None] - 1
    last_gate = jnp.sum(jnp.where(is_last, cache_gates, jnp.float32(0.0)), axis=-1)
    new_gate = last_gate + log_gate
    scores = (
        jnp.einsum("shd,shld->shl", query, cache_keys, preferred_element_type=jnp.float32) * scale
    )
    scores = scores + (new_gate[..., None] - cache_gates)
    scores = jnp.where(valid, scores, -jnp.inf)
    own_score = jnp.sum(query.astype(jnp.float32) * key_new.astype(jnp.float32), axis=-1) * scale
    highest = jnp.maximum(jnp.max(scores, axis=-1), own_score)
    cached_weight = jnp.exp(scores - highest[..., None])
    own_weight = jnp.exp(own_score - highest)
    denominator = jnp.sum(cached_weight, axis=-1) + own_weight
    cached_share = (cached_weight / denominator[..., None]).astype(jnp.bfloat16)
    attended = jnp.einsum(
        "shl,shld->shd", cached_share, cache_values, preferred_element_type=jnp.float32
    )
    attended = attended + (own_weight / denominator)[..., None] * value_new.astype(jnp.float32)
    attended = attended.astype(jnp.bfloat16).reshape(seq_count, inner)
    head_terms = jnp.dot(
        attended, gathered_copies(w_out, "ep", 1), preferred_element_type=jnp.float32
    )
    residual = tokens.astype(jnp.float32) + taken_together(head_terms, "tp")
    normed_two = rms_norm(residual, moe_gain)
    top_count = routing.shape[1]
    expert_count = lax.axis_size("ep") * w_gate.shape[0]
    capacity = max(1, 2 * seq_count * top_count // expert_count)
    flat = routing.reshape(-1)
    onehot = (flat[:, None] == jnp.arange(expert_count, dtype=jnp.int32)[None, :]).astype(jnp.int32)
    earlier = jnp.cumsum(onehot, axis=0) - onehot
    slot_index = jnp.sum(earlier * onehot, axis=1)
    target = flat * capacity + slot_index
    selector = (
        jnp.arange(expert_count * capacity, dtype=jnp.int32)[:, None] == target[None, :]
    ).astype(jnp.bfloat16)
    repeated = jnp.repeat(normed_two, top_count, axis=0)
    narrow = model_width // lax.axis_size("tp")
    offset = lax.axis_index("tp") * narrow
    repeated_part = lax.dynamic_slice_in_dim(repeated, offset, narrow, 1)
    send_part = jnp.dot(selector, repeated_part, preferred_element_type=jnp.float32).astype(
        jnp.bfloat16
    )
    send_part = send_part.reshape(expert_count, capacity, narrow)
    received = lax.all_to_all(send_part, "ep", split_axis=0, concat_axis=0, tiled=True)
    sources = received.shape[0]
    slots_here = received.shape[1]
    full_rows = gathered_copies(received, "tp", 2)
    partial_out = expert_partial(
        full_rows.reshape(-1, model_width), gate_matrix, up_matrix, down_matrix
    )
    partial_out = partial_out.reshape(sources, slots_here, model_width)
    summed = sum_at_owner(partial_out, "tp", 2)
    served = summed.astype(jnp.bfloat16)
    returned = lax.all_to_all(served, "ep", split_axis=0, concat_axis=0, tiled=True)
    gathered = jnp.take(returned.reshape(-1, narrow), target, axis=0).astype(jnp.float32)
    gathered = gathered.reshape(seq_count, top_count, narrow)
    expert_sum = jnp.sum(route_weight[..., None] * gathered, axis=1)
    residual_part = lax.dynamic_slice_in_dim(residual, offset, narrow, 1)
    out_part = (residual_part + expert_sum).astype(jnp.bfloat16)
    return gathered_copies(out_part, "tp", 1)


def solution(mesh):
    in_specs = (
        P("ep", None),
        P(),
        P("ep", "tp"),
        P("ep", "tp"),
        P("ep", "tp"),
        P("ep", "tp"),
        P("tp"),
        P("ep", "tp", None, None),
        P("ep", "tp", None, None),
        P("ep", "tp", None),
        P("ep"),
        P("tp", "ep"),
        P(),
        P("ep", None),
        P("ep", None),
        P("ep", None, "tp"),
        P("ep", None, "tp"),
        P("ep", "tp", None),
    )
    out_specs = P("ep", None)
    return jax.shard_map(local, mesh=mesh, in_specs=in_specs, out_specs=out_specs, check_vma=False)
```

profile of v0, /device:TPU:1, one launch (start us, length us, event | category | flops | bytes accessed | tf_op | source)
XLA Modules:
  0.0 200.2 jit_solution(7899206140547130557)
XLA Ops:
  0.0 1.0 broadcast_in_dim.27
  1.0 1.1 reshape.263
  2.1 16.7 %all-to-all-start = ((bf16[32,2,2048]{2,1,0:T(2,128)(2,1)}), bf16[32,2,2048]{2,1,0:T(2,128)(2,1)S(1)}, u32[]{:S(2)}, u32[]{:S(2)}) async-start(bf16[32,2,2048]{2,1,0:T(2,128)(2,1)} %reshape.263), calls=%async_computation | async-start | bytes 524288 | tf_op jit(solution)/shard_map/all_to_all | solution.py:20
  18.8 0.8 copy.75
  19.6 0.8 pad_maximum_fusion
  20.4 0.0 copy-start.8
  20.5 0.0 copy-start.2
  20.5 40.0 %all_gather.3 = bf16[2048,193]{1,0:T(8,128)(2,1)S(1)} all-gather(bf16[64,193]{1,0:T(8,128)(2,1)S(1)} %pad_maximum_fusion), channel_id=1, replica_groups=mesh['ep'=32,'tp'=16] {'ep'}, dimensions={0}, use_global_device_ids=true | all-gather | bytes 815232 | tf_op jit(solution)/shard_map/all_gather | solution.py:14
  60.5 0.1 fusion.15
  60.6 0.3 fusion.45
  60.9 0.0 copy-done
  60.9 0.4 fusion.2
  61.4 0.3 fusion.25
  61.7 0.1 copy.76
  62.4 0.2 fusion.33
  62.6 0.3 fusion.44
  63.0 0.2 multiply_reduce_fusion.2
  63.1 0.3 fusion.43
  63.5 2.3 %fusion = f32[16,1,64]{2,1,0:T(1,128)S(1)} fusion(bf16[16,1,1024,64]{2,3,1,0:T(8,128)(2,1)} %param.26, f32[16]{0:T(128)S(1)} %get-tuple-element.10, f32[16,1,1024]{2,1,0:T(1,128)S(1)} %get-tuple-element.8, f32[16]{0:T(128)S(1)} %multiply_maximum_fusion), kind=kOutput, calls=%fused_computation.1 | convolution fusion | flops 2146304 | bytes 2166912 | tf_op jit(solution)/shard_map/shl,shld->shd/dot_general | solution.py:134
  65.8 0.0 all-to-all-done
  65.8 0.4 reshape.264
  66.2 0.3 copy.77
  66.5 0.5 reshape.241
  67.0 0.2 fusion.36
  67.2 1.5 broadcast_in_dim.28
  68.8 6.9 %all-to-all-start.1 = ((f32[16,16,2048]{2,1,0:T(8,128)}), f32[16,16,2048]{2,1,0:T(8,128)}, u32[]{:S(2)}, u32[]{:S(2)}) async-start(f32[16,16,2048]{2,1,0:T(8,128)} %broadcast_in_dim.28), calls=%async_computation.1 | async-start | bytes 4194304 | tf_op jit(solution)/shard_map/all_to_all | solution.py:20
  75.7 0.0 copy-done.6
  75.7 0.1 copy.79
  75.8 0.1 reshape.242
  75.9 0.1 fusion.29
  76.0 0.1 reduce_window_sum.11
  76.1 0.2 select_reduce_fusion
  76.3 32.3 %all-to-all-done.1 = f32[16,16,2048]{2,1,0:T(8,128)} async-done(((f32[16,16,2048]{2,1,0:T(8,128)}), f32[16,16,2048]{2,1,0:T(8,128)}, u32[]{:S(2)}, u32[]{:S(2)}) %all-to-all-start.1) | async-done | bytes 2097184 | tf_op jit(solution)/shard_map/all_to_all | solution.py:20
  108.6 1.7 reduce_sum.92
  110.3 0.0 copy-start.9
  110.3 0.1 multiply_reduce_fusion
  110.5 0.1 multiply_convert_fusion
  110.6 0.1 broadcast_in_dim.30
  110.7 0.0 copy-start.10
  110.7 0.1 reshape.243
  110.7 0.1 convolution_convert_fusion
  110.9 23.6 %all_to_all.35 = bf16[32,4,128]{2,1,0:T(4,128)(2,1)S(1)} all-to-all(bf16[32,4,128]{2,1,0:T(4,128)(2,1)S(1)} %bitcast.73), channel_id=1, replica_groups=mesh['ep'=32,'tp'=16] {'ep'}, dimensions={0} | all-to-all | bytes 65536 | tf_op jit(solution)/shard_map/all_to_all | solution.py:163
  134.5 0.2 broadcast_in_dim.31
  134.7 0.0 copy-start.3
  134.7 13.5 %all_to_all.36 = bf16[16,32,4,128]{3,2,1,0:T(4,128)(2,1)S(1)} all-to-all(bf16[16,32,4,128]{3,2,1,0:T(4,128)(2,1)S(1)} %broadcast_in_dim.31), channel_id=1, replica_groups=mesh['ep'=32,'tp'=16] {'tp'}, dimensions={0} | all-to-all | bytes 1048576 | tf_op jit(solution)/shard_map/all_to_all | solution.py:20
  148.2 0.6 copy.81
  148.8 0.3 convolution_minimum_fusion
  149.1 0.3 fusion.7
  149.4 0.1 copy.82
  149.6 0.3 convolution_bitcast_fusion
  149.9 1.1 copy.85
  150.9 3.8 %all-to-all-start.4 = ((f32[16,32,4,128]{3,1,2,0:T(8,128)}), f32[16,32,4,128]{3,1,2,0:T(8,128)S(1)}, u32[]{:S(2)}, u32[]{:S(2)}) async-start(f32[16,32,4,128]{3,1,2,0:T(8,128)} %copy.85), calls=%async_computation.4 | async-start | bytes 2097152 | tf_op jit(solution)/shard_map/all_to_all | solution.py:49
  154.7 0.1 reduce_sum.94
  154.8 0.1 mul.158
  154.9 14.7 %all-to-all-done.4 = f32[16,32,4,128]{3,1,2,0:T(8,128)S(1)} async-done(((f32[16,32,4,128]{3,1,2,0:T(8,128)}), f32[16,32,4,128]{3,1,2,0:T(8,128)S(1)}, u32[]{:S(2)}, u32[]{:S(2)}) %all-to-all-start.4) | async-done | bytes 1048608 | tf_op jit(solution)/shard_map/all_to_all | solution.py:49
  169.6 0.1 reduce_sum.96
  169.7 0.6 copy.87
  170.3 7.1 %all-to-all-start.5 = ((bf16[32,4,128]{2,1,0:T(4,128)(2,1)}), bf16[32,4,128]{2,1,0:T(4,128)(2,1)S(1)}, u32[]{:S(2)}, u32[]{:S(2)}) async-start(bf16[32,4,128]{2,1,0:T(4,128)(2,1)} %copy.87), calls=%async_computation.5 | async-start | bytes 65536 | tf_op jit(solution)/shard_map/all_to_all | solution.py:173
  177.4 0.1 copy.78
  177.5 12.1 %all-to-all-done.5 = bf16[32,4,128]{2,1,0:T(4,128)(2,1)S(1)} async-done(((bf16[32,4,128]{2,1,0:T(4,128)(2,1)}), bf16[32,4,128]{2,1,0:T(4,128)(2,1)S(1)}, u32[]{:S(2)}, u32[]{:S(2)}) %all-to-all-start.5) | async-done | bytes 32800 | tf_op jit(solution)/shard_map/all_to_all | solution.py:173
  189.7 0.6 gather_fusion
  190.3 0.1 multiply_reduce_fusion.1
  190.4 9.2 %all_to_all.37 = bf16[16,16,128]{2,1,0:T(8,128)(2,1)S(1)} all-to-all(bf16[16,16,128]{2,1,0:T(8,128)(2,1)S(1)} %broadcast_in_dim.33), channel_id=1, replica_groups=mesh['ep'=32,'tp'=16] {'tp'}, dimensions={0} | all-to-all | bytes 131072 | tf_op jit(solution)/shard_map/all_to_all | solution.py:20
  199.6 0.6 copy_bitcast_fusion
  (31 shorter events, 0.2 us)
Async XLA Ops:
  0.0 60.9 %copy-start = (bf16[16,1,1024,64]{2,3,1,0:T(8,128)(2,1)S(1)}, bf16[16,1,1024,64]{2,3,1,0:T(8,128)(2,1)}, u32[]{:S(2)}) copy-start(bf16[16,1,1024,64]{2,3,1,0:T(8,128)(2,1)} %param.25) | copy-start | bytes 6291460
  0.0 60.5 %copy-start.4 = (bf16[2048]{0:T(1024)(128)(2,1)S(1)}, bf16[2048]{0:T(1024)(128)(2,1)}, u32[]{:S(2)}) copy-start(bf16[2048]{0:T(1024)(128)(2,1)} %param.19) | copy-start | bytes 12292
  0.0 60.5 %copy-start.1 = (bf16[16,2048]{1,0:T(8,128)(2,1)S(1)}, bf16[16,2048]{1,0:T(8,128)(2,1)}, u32[]{:S(2)}) copy-start(bf16[16,2048]{1,0:T(8,128)(2,1)} %param.18) | copy-start | bytes 196612
  2.1 63.7 %all-to-all-start = ((bf16[32,2,2048]{2,1,0:T(2,128)(2,1)}), bf16[32,2,2048]{2,1,0:T(2,128)(2,1)S(1)}, u32[]{:S(2)}, u32[]{:S(2)}) async-start(bf16[32,2,2048]{2,1,0:T(2,128)(2,1)} %reshape.263), calls=%async_computation | async-start | bytes 524288 | tf_op jit(solution)/shard_map/all_to_all | solution.py:20
  20.4 40.9 %copy-start.8 = (s32[16]{0:T(128)S(1)}, s32[16]{0:T(128)}, u32[]{:S(2)}) copy-start(s32[16]{0:T(128)} %param.28) | copy-start | bytes 196
  20.5 40.9 %copy-start.2 = (f32[16,1,1024]{2,1,0:T(1,128)S(1)}, f32[16,1,1024]{2,1,0:T(1,128)}, u32[]{:S(2)}) copy-start(f32[16,1,1024]{2,1,0:T(1,128)} %param.27) | copy-start | bytes 196612
  68.8 7.0 %copy-start.5 = (bf16[2048]{0:T(1024)(128)(2,1)S(1)}, bf16[2048]{0:T(1024)(128)(2,1)}, u32[]{:S(2)}) copy-start(bf16[2048]{0:T(1024)(128)(2,1)} %param.30) | copy-start | bytes 12292
  68.8 7.0 %copy-start.6 = (s32[16,4]{0,1:T(4,128)S(1)}, s32[16,4]{0,1:T(4,128)}, u32[]{:S(2)}) copy-start(s32[16,4]{0,1:T(4,128)} %param.31) | copy-start | bytes 772
  68.8 39.8 %all-to-all-start.1 = ((f32[16,16,2048]{2,1,0:T(8,128)}), f32[16,16,2048]{2,1,0:T(8,128)}, u32[]{:S(2)}, u32[]{:S(2)}) async-start(f32[16,16,2048]{2,1,0:T(8,128)} %broadcast_in_dim.28), calls=%async_computation.1 | async-start | bytes 4194304 | tf_op jit(solution)/shard_map/all_to_all | solution.py:20
  110.3 38.5 %copy-start.9 = (bf16[1,2048,64]{1,2,0:T(8,128)(2,1)S(1)}, bf16[1,2048,64]{1,2,0:T(8,128)(2,1)}, u32[]{:S(2)}) copy-start(bf16[1,2048,64]{1,2,0:T(8,128)(2,1)} %param.33) | copy-start | bytes 786436
  110.7 38.5 %copy-start.10 = (bf16[1,2048,64]{1,2,0:T(8,128)(2,1)S(1)}, bf16[1,2048,64]{1,2,0:T(8,128)(2,1)}, u32[]{:S(2)}) copy-start(bf16[1,2048,64]{1,2,0:T(8,128)(2,1)} %param.34) | copy-start | bytes 786436
  134.7 14.9 %copy-start.3 = (bf16[1,64,2048]{2,1,0:T(8,128)(2,1)S(1)}, bf16[1,64,2048]{2,1,0:T(8,128)(2,1)}, u32[]{:S(2)}) copy-start(bf16[1,64,2048]{2,1,0:T(8,128)(2,1)} %param.35) | copy-start | bytes 786436
  150.9 26.5 %copy-start.7 = (f32[16,4]{0,1:T(4,128)S(1)}, f32[16,4]{0,1:T(4,128)}, u32[]{:S(2)}) copy-start(f32[16,4]{0,1:T(4,128)} %param.32) | copy-start | bytes 772
  150.9 18.6 %all-to-all-start.4 = ((f32[16,32,4,128]{3,1,2,0:T(8,128)}), f32[16,32,4,128]{3,1,2,0:T(8,128)S(1)}, u32[]{:S(2)}, u32[]{:S(2)}) async-start(f32[16,32,4,128]{3,1,2,0:T(8,128)} %copy.85), calls=%async_computation.4 | async-start | bytes 2097152 | tf_op jit(solution)/shard_map/all_to_all | solution.py:49
  170.3 19.4 %all-to-all-start.5 = ((bf16[32,4,128]{2,1,0:T(4,128)(2,1)}), bf16[32,4,128]{2,1,0:T(4,128)(2,1)S(1)}, u32[]{:S(2)}, u32[]{:S(2)}) async-start(bf16[32,4,128]{2,1,0:T(4,128)(2,1)} %copy.87), calls=%async_computation.5 | async-start | bytes 65536 | tf_op jit(solution)/shard_map/all_to_all | solution.py:173
where the time goes:
time: 201 us; the launch traced here: 200 us
  blocking collectives  86.2 us (43%)
  waiting for transfers between devices  59.1 us (29%)
  starting transfers between devices  34.5 us (17%)
  local copies, waits for them, and re-layouts  10.2 us (5%)
  other arithmetic  4.9 us (2%)
  matrix products  4.23 us (2%)
    all_gather x1, blocking collectives, sent_together(): result = lax.all_gather(both, axis, axis=dim, tiled=True)  40 us
    all_to_all x2, waiting for transfers between devices, from_everyone(): lax.all_to_all(jnp.broadcast_to(shard[None], (size, *shard.shape)), axis,...  32.3 us
    all_to_all x2, starting transfers between devices, from_everyone(): lax.all_to_all(jnp.broadcast_to(shard[None], (size, *shard.shape)), axis,...  23.7 us
    all_to_all x1, blocking collectives, local(): lax.all_to_all(send_part, 'ep', split_axis=0, concat_axis=0, tiled=True)  23.6 us
    all_to_all x2, blocking collectives, from_everyone(): lax.all_to_all(jnp.broadcast_to(shard[None], (size, *shard.shape)), axis,...  22.7 us
    all_to_all x1, waiting for transfers between devices, sum_at_owner(): tiles = lax.all_to_all(split_up(shard, dim, size), axis, 0, 0, tiled=True)  14.7 us
    all_to_all x1, waiting for transfers between devices, local(): lax.all_to_all(served, 'ep', split_axis=0, concat_axis=0, tiled=True)  12.1 us
    all_to_all x1, starting transfers between devices, local(): lax.all_to_all(served, 'ep', split_axis=0, concat_axis=0, tiled=True)  7.09 us
  transfers between devices with their start and end apart: 4, of which 3 were waited for; matrix products, arithmetic and copies ran while one was open for 4% of the time, Pallas kernels for 0%

commit v1 on v0

v1 whole, which is shorter than its diff:
```python
import jax
import jax.numpy as jnp
from jax import lax
from jax.sharding import PartitionSpec as P

NORM_EPSILON = 1e-06
CLAMP_LIMIT = 7.0
SIGMOID_SLOPE = 1.702
F32 = jnp.float32
BF16 = jnp.bfloat16


def to_everyone(shard, axis):
    size = lax.axis_size(axis)
    return lax.all_to_all(
        jnp.broadcast_to(shard[None], (size, *shard.shape)), axis, 0, 0, tiled=True
    )


def local(
    tokens,
    attn_gain,
    w_query,
    w_key,
    w_value,
    w_forget,
    forget_bias,
    cache_keys,
    cache_values,
    cache_gates,
    lengths,
    w_out,
    moe_gain,
    routing,
    route_weight,
    w_gate,
    w_up,
    w_down,
):
    n_ep = lax.axis_size("ep")
    n_tp = lax.axis_size("tp")
    rows, width = tokens.shape
    head = cache_keys.shape[3]
    chips = n_ep // 2
    block = width // n_ep
    narrow = width // n_tp
    core = lax.axis_index("ep") % 2
    offset = lax.axis_index("tp") * narrow

    packed = jnp.concatenate([w_query, w_key, w_value, w_out.T, w_forget], axis=1)
    same_core = [[2 * z + c for z in range(chips)] for c in range(2)]
    mine = lax.all_gather(packed, "ep", axis=0, tiled=True, axis_index_groups=same_core)
    theirs = lax.ppermute(mine, "ep", [(i, i ^ 1) for i in range(n_ep)])

    wide = tokens.astype(F32)
    normed = wide * lax.rsqrt(jnp.mean(wide * wide, axis=-1, keepdims=True) + NORM_EPSILON)
    normed = (normed * attn_gain.astype(F32)).astype(BF16)
    by_core = normed.reshape(rows, chips, 2, block)
    even = by_core[:, :, 0].reshape(rows, chips * block)
    odd = by_core[:, :, 1].reshape(rows, chips * block)
    is_odd = core == 1
    first = jnp.where(is_odd, theirs, mine)
    second = jnp.where(is_odd, mine, theirs)
    projected = jnp.dot(even, first, preferred_element_type=F32) + jnp.dot(
        odd, second, preferred_element_type=F32
    )
    query = projected[:, :head].astype(BF16)
    key_new = projected[:, head : 2 * head].astype(BF16)
    value_new = projected[:, 2 * head : 3 * head].astype(BF16)
    log_gate = jax.nn.log_sigmoid(projected[:, 4 * head] + forget_bias[0])

    keys = cache_keys[:, 0]
    values = cache_values[:, 0]
    gates = cache_gates[:, 0]
    scale = head ** (-0.5)
    positions = jnp.arange(keys.shape[1], dtype=jnp.int32)
    valid = positions[None, :] < lengths[:, None]
    is_last = positions[None, :] == lengths[:, None] - 1
    last_gate = jnp.sum(jnp.where(is_last, gates, F32(0.0)), axis=-1)
    new_gate = last_gate + log_gate
    scores = jnp.einsum("sd,sld->sl", query, keys, preferred_element_type=F32) * scale
    scores = scores + (new_gate[:, None] - gates)
    scores = jnp.where(valid, scores, -jnp.inf)
    own_score = jnp.sum(query.astype(F32) * key_new.astype(F32), axis=-1) * scale
    highest = jnp.maximum(jnp.max(scores, axis=-1), own_score)
    cached_weight = jnp.exp(scores - highest[:, None])
    own_weight = jnp.exp(own_score - highest)
    denominator = jnp.sum(cached_weight, axis=-1) + own_weight
    share = (cached_weight / denominator[:, None]).astype(BF16)
    attended = jnp.einsum("sl,sld->sd", share, values, preferred_element_type=F32)
    attended = attended + (own_weight / denominator)[:, None] * value_new.astype(F32)
    attended = attended.astype(BF16)

    out_first = first[:, 3 * head : 4 * head].reshape(chips, block, head)
    out_second = second[:, 3 * head : 4 * head].reshape(chips, block, head)
    out_blocks = jnp.concatenate([out_first, out_second], axis=1)
    head_terms = jnp.einsum("sd,zfd->zsf", attended, out_blocks, preferred_element_type=F32)
    parts = lax.all_to_all(head_terms, "tp", 0, 0, tiled=True)
    residual = lax.dynamic_slice_in_dim(tokens, offset, narrow, 1).astype(F32) + jnp.sum(parts, axis=0)

    top = routing.shape[1]
    capacity = max(1, 2 * rows * top // n_ep)
    flat = routing.reshape(-1)
    order = jnp.arange(rows * top, dtype=jnp.int32)
    same = (flat[:, None] == flat[None, :]) & (order[None, :] < order[:, None])
    target = flat * capacity + jnp.sum(same.astype(jnp.int32), axis=1)
    slots = n_ep * capacity
    hits = jnp.arange(slots, dtype=jnp.int32)[:, None, None] == target.reshape(rows, top)[None]
    selector = jnp.any(hits, axis=2).astype(BF16)
    mix = jnp.sum(jnp.where(hits, route_weight[None], F32(0.0)), axis=2)

    gain_here = lax.dynamic_slice_in_dim(moe_gain, offset, narrow, 0).astype(F32)
    scaled = (residual * gain_here).astype(BF16)
    squares = jnp.sum(residual * residual, axis=1)
    high = squares.astype(BF16)
    low = (squares - high.astype(F32)).astype(BF16)
    lane = jnp.arange(narrow, dtype=jnp.int32)[None, :]
    marks = jnp.where(lane == 0, high[:, None], jnp.where(lane == 1, low[:, None], BF16(0)))
    chosen = jnp.dot(selector, jnp.concatenate([scaled, marks], axis=1), preferred_element_type=F32)
    chosen = chosen.astype(BF16)
    sent = jnp.concatenate(
        [
            chosen[:, :narrow].reshape(n_ep, capacity, narrow),
            chosen[:, narrow:].reshape(n_ep, capacity, narrow),
        ],
        axis=1,
    )
    received = lax.all_to_all(sent, "ep", 0, 0, tiled=True)
    slices = received[:, :capacity].reshape(slots, narrow)
    marks_in = received[:, capacity:, :2].reshape(slots, 2)
    marks_rows = jnp.pad(marks_in.T, ((0, 14), (0, narrow - slots))) if slots <= narrow else None
    gathered = to_everyone(jnp.concatenate([slices, marks_rows], axis=0), "tp")
    full = gathered[:, :slots]
    total = jnp.sum(gathered[:, slots : slots + 2, :slots].astype(F32), axis=(0, 1))
    row_scale = lax.rsqrt(total / width + NORM_EPSILON)

    gate_pre = jnp.einsum(
        "trf,tfu->ru", full, w_gate[0].reshape(n_tp, narrow, -1), preferred_element_type=F32
    ) * row_scale[:, None]
    up_pre = jnp.einsum(
        "trf,tfu->ru", full, w_up[0].reshape(n_tp, narrow, -1), preferred_element_type=F32
    ) * row_scale[:, None]
    gate_cut = jnp.minimum(gate_pre, CLAMP_LIMIT)
    up_cut = jnp.clip(up_pre, -CLAMP_LIMIT, CLAMP_LIMIT)
    hidden = ((up_cut + 1.0) * gate_cut * jax.nn.sigmoid(SIGMOID_SLOPE * gate_cut)).astype(BF16)
    down = w_down[0].reshape(-1, n_tp, narrow)
    partial = jnp.einsum("ru,utf->trf", hidden, down, preferred_element_type=F32).astype(BF16)
    partial = lax.all_to_all(partial, "tp", 0, 0, tiled=True)
    served = jnp.sum(partial.astype(F32), axis=0).astype(BF16)

    returned = lax.all_to_all(served.reshape(n_ep, capacity, narrow), "ep", 0, 0, tiled=True)
    expert_sum = lax.dot_general(
        mix,
        returned.reshape(slots, narrow).astype(F32),
        (((0,), (0,)), ((), ())),
        precision=lax.Precision.HIGHEST,
        preferred_element_type=F32,
    )
    out_part = (residual + expert_sum).astype(BF16)
    final = to_everyone(out_part, "tp")
    return jnp.moveaxis(final, 0, 1).reshape(rows, width)


def solution(mesh):
    in_specs = (
        P("ep", None),
        P(),
        P("ep", "tp"),
        P("ep", "tp"),
        P("ep", "tp"),
        P("ep", "tp"),
        P("tp"),
        P("ep", "tp", None, None),
        P("ep", "tp", None, None),
        P("ep", "tp", None),
        P("ep"),
        P("tp", "ep"),
        P(),
        P("ep", None),
        P("ep", None),
        P("ep", None, "tp"),
        P("ep", None, "tp"),
        P("ep", "tp", None),
    )
    out_specs = P("ep", None)
    return jax.shard_map(local, mesh=mesh, in_specs=in_specs, out_specs=out_specs, check_vma=False)
```

time: 201 us -> 163 us (0.81)
  waiting for transfers between devices: 59.1 us -> 26.5 us
  blocking collectives: 86.2 us -> 76 us
  starting transfers between devices: 34.5 us -> 27.2 us
  local copies, waits for them, and re-layouts: 10.2 us -> 15 us
  matrix products: 4.23 us -> 8 us
  other arithmetic: 4.9 us -> 8.14 us
    all_to_all x4 -> x3, waiting for transfers between devices: 59.1 us -> 26.5 us  [the longest x1 12 us: local(): lax.all_to_all(served.reshape(n_ep, capacity, narrow), 'ep', 0, 0, tiled=...]
    all_to_all x4 -> x3, starting transfers between devices: 34.5 us -> 17.6 us  [the longest x1 7.23 us: local(): lax.all_to_all(served.reshape(n_ep, capacity, narrow), 'ep', 0, 0, tiled=...]
    ppermute x0 -> x1, starting transfers between devices: none -> 9.63 us  [local(): theirs = lax.ppermute(mine, 'ep', [(i, i ^ 1) for i in range(n_ep)])]
    all_gather x1, blocking collectives: 40 us -> 33.9 us  [local(): lax.all_gather(packed, 'ep', axis=0, tiled=True, axis_index_groups=same_c...]
    all_to_all x3, blocking collectives: 46.2 us -> 42.1 us  [the longest x1 20.6 us: local(): received = lax.all_to_all(sent, 'ep', 0, 0, tiled=True)]
    dot_general x8 -> x9, matrix products: 4.23 us -> 8 us  [the longest x1 2.23 us: local(): jnp.einsum('sl,sld->sd', share, values, preferred_element_type=F32)]
    unnamed x27 -> x22, local copies, waits for them, and re-layouts: 2.45 us -> 4.98 us
    convert_element_type x5 -> x6, other arithmetic: 0.18 us -> 2.4 us  [the longest x1 0.81 us: local(): scaled = (residual * gain_here).astype(BF16)]
  transfers between devices with their start and end apart: 4 -> 4, of which waited for: 3 -> 3; matrix products, arithmetic and copies ran while one was open for 4% -> 8% of each run, Pallas kernels for 0% -> 0%
where the time goes in v1:
time: 163 us; the launch traced here: 162 us
  blocking collectives  76 us (47%)
  starting transfers between devices  27.2 us (17%)
  waiting for transfers between devices  26.5 us (16%)
  local copies, waits for them, and re-layouts  15 us (9%)
  other arithmetic  8.14 us (5%)
  matrix products  8 us (5%)
    all_gather x1, blocking collectives, local(): lax.all_gather(packed, 'ep', axis=0, tiled=True, axis_index_groups=same_c...  33.9 us
    all_to_all x1, blocking collectives, local(): received = lax.all_to_all(sent, 'ep', 0, 0, tiled=True)  20.6 us
    all_to_all x1, blocking collectives, local(): partial = lax.all_to_all(partial, 'tp', 0, 0, tiled=True)  12.4 us
    all_to_all x1, waiting for transfers between devices, local(): lax.all_to_all(served.reshape(n_ep, capacity, narrow), 'ep', 0, 0, tiled=...  12 us
    ppermute x1, starting transfers between devices, local(): theirs = lax.ppermute(mine, 'ep', [(i, i ^ 1) for i in range(n_ep)])  9.63 us
    all_to_all x1, blocking collectives, to_everyone(): lax.all_to_all(jnp.broadcast_to(shard[None], (size, *shard.shape)), axis,...  9.19 us
    all_to_all x1, waiting for transfers between devices, to_everyone(): lax.all_to_all(jnp.broadcast_to(shard[None], (size, *shard.shape)), axis,...  8.26 us
    all_to_all x1, starting transfers between devices, local(): lax.all_to_all(served.reshape(n_ep, capacity, narrow), 'ep', 0, 0, tiled=...  7.23 us
  transfers between devices with their start and end apart: 4, of which 3 were waited for; matrix products, arithmetic and copies ran while one was open for 8% of the time, Pallas kernels for 0%

profile of v1, /device:TPU:1, one launch (start us, length us, event | category | flops | bytes accessed | tf_op | source)
XLA Modules:
  0.0 161.9 jit_solution(5556839501885827413)
XLA Ops:
  0.0 1.0 copy.116
  1.0 0.8 copy.117
  1.7 0.9 concatenate.15
  2.6 33.9 %all_gather.3 = bf16[1024,257]{1,0:T(8,128)(2,1)S(1)} all-gather(bf16[64,257]{1,0:T(8,128)(2,1)S(1)} %concatenate.15), channel_id=1, replica_groups={{0,32,64,96,128,160,192,224,256,288,320,352,384,416,448,480},{16,48,80,..., dimensions={0}, use_global_device_ids=true | all-gather | bytes 559232 | tf_op jit(solution)/shard_map/all_gather | solution.py:52
  36.5 1.0 copy.118
  37.5 9.6 %collective-permute-start = (bf16[1024,257]{0,1:T(8,128)(2,1)}, bf16[1024,257]{0,1:T(8,128)(2,1)S(1)}, u32[]{:S(2)}, u32[]{:S(2)}) collective-permute-start(bf16[1024,257]{0,1:T(8,128)(2,1)} %copy.118), channel_id=1, source_target_pairs={{0,16},{16,0},{32,48},{48,32},{64,80},{80,64},{96,112},{112,96},{1... | collective-permute-start | bytes 1579016 | tf_op jit(solution)/shard_map/ppermute | solution.py:53
  47.2 0.1 fusion.25
  47.3 0.7 fusion.27
  48.1 1.0 reshape.103
  49.1 1.4 slice_reduce_fusion.1
  50.5 1.0 reshape_squeeze.16
  51.4 1.0 reshape_squeeze.15
  52.4 0.7 broadcast_add_fusion
  53.1 1.0 fusion.29
  54.1 0.1 copy.127
  54.8 0.8 copy.128
  55.6 0.1 eq.70
  55.7 0.2 convert_reduce_fusion
  55.9 0.1 reduce_sum.104
  55.9 0.1 copy.129
  56.0 0.7 multiply_add_fusion
  56.7 0.0 collective-permute-done
  56.7 1.2 copy.119
  57.9 1.3 broadcast_select_fusion.1
  59.2 0.2 fusion.73
  59.4 0.0 copy-start.2
  59.4 0.0 copy-start.7
  59.4 0.2 fusion.72
  59.6 0.2 multiply_reduce_fusion.1
  59.8 0.1 slice.65
  60.0 0.1 slice.66
  60.1 0.4 fusion.2
  60.5 0.1 fusion.50
  60.6 0.2 fusion.68
  60.8 0.2 fusion.33
  61.1 0.1 fusion.41
  61.2 0.2 copy.123
  61.3 0.2 copy.124
  61.5 2.2 %fusion = f32[16,1,64]{2,1,0:T(1,128)S(1)} fusion(bf16[16,1,1024,64]{2,3,1,0:T(8,128)(2,1)} %param.26, bf16[16,1024,1]{1,0,2:T(8,128)(2,1)S(1)} %fusion.41), kind=kOutput, calls=%fused_computation | convolution fusion | flops 2097152 | bytes 2134016 | tf_op jit(solution)/shard_map/sl,sld->sd/dot_general | solution.py:90
  63.8 0.9 convolution_bitcast_fusion
  64.7 6.8 %all-to-all-start = ((f32[16,16,128]{2,1,0:T(8,128)}), f32[16,16,128]{2,1,0:T(8,128)S(1)}, u32[]{:S(2)}, u32[]{:S(2)}) async-start(f32[16,16,128]{2,1,0:T(8,128)} %convolution_bitcast_fusion), calls=%async_computation | async-start | bytes 262144 | tf_op jit(solution)/shard_map/all_to_all | solution.py:98
  71.4 0.8 dynamic-slice_convert_fusion
  72.2 0.1 fusion.40
  72.3 6.3 %all-to-all-done = f32[16,16,128]{2,1,0:T(8,128)S(1)} async-done(((f32[16,16,128]{2,1,0:T(8,128)}), f32[16,16,128]{2,1,0:T(8,128)S(1)}, u32[]{:S(2)}, u32[]{:S(2)}) %all-to-all-start) | async-done | bytes 131104 | tf_op jit(solution)/shard_map/all_to_all | solution.py:98
  78.6 0.8 multiply_convert_fusion
  79.4 0.1 select_select_fusion
  79.5 0.2 convolution_convert_fusion.1
  79.8 20.6 %all_to_all.30 = bf16[32,8,128]{2,1,0:T(8,128)(2,1)S(1)} all-to-all(bf16[32,8,128]{2,1,0:T(8,128)(2,1)S(1)} %pad_maximum_fusion), channel_id=1, replica_groups=mesh['ep'=32,'tp'=16] {'ep'}, dimensions={0} | all-to-all | bytes 131072 | tf_op jit(solution)/shard_map/all_to_all | solution.py:128
  100.4 0.1 copy.130
  100.5 0.9 broadcast_in_dim.97
  101.4 3.6 %all-to-all-start.2 = ((bf16[16,144,128]{2,1,0:T(8,128)(2,1)}), bf16[16,144,128]{2,1,0:T(8,128)(2,1)S(1)}, u32[]{:S(2)}, u32[]{:S(2)}) async-start(bf16[16,144,128]{2,1,0:T(8,128)(2,1)} %broadcast_in_dim.97), calls=%async_computation.2 | async-start | bytes 1179648 | tf_op jit(solution)/shard_map/all_to_all | solution.py:15
  105.0 0.7 copy.148
  105.8 1.7 %copy.149 = bf16[8,8,16,128]{3,2,1,0:T(8,128)(2,1)} copy(bf16[8,8,16,128]{3,1,2,0:T(8,128)(2,1)} %bitcast.107) | data formatting | bytes 524288
  107.5 8.3 %all-to-all-done.2 = bf16[16,144,128]{2,1,0:T(8,128)(2,1)S(1)} async-done(((bf16[16,144,128]{2,1,0:T(8,128)(2,1)}), bf16[16,144,128]{2,1,0:T(8,128)(2,1)S(1)}, u32[]{:S(2)}, u32[]{:S(2)}) %all-to-all-start.2) | async-done | bytes 589856 | tf_op jit(solution)/shard_map/all_to_all | solution.py:15
  115.8 1.3 fusion.6
  117.0 1.8 %fusion.4 = bf16[16,128,128]{2,1,0:T(8,128)(2,1)S(1)} fusion(f32[128,64]{0,1:T(8,128)S(1)} %fusion.6, bf16[16,144,128]{2,1,0:T(8,128)(2,1)S(1)} %all-to-all-done.2, bf16[64,16,128]{2,1,0:T(8,128)(2,1)} %bitcast.104, bf16[16,128,64]{1,0,2:T(8,128)(2,1)S(1)} %bitcast.103, f32[128]{0:T(128)S(1)} %add_rsqrt_fusion), kind=kOutput, calls=%fused_computation.5 | convolution fusion | flops 67452928 | bytes 1606144 | tf_op jit(solution)/shard_map/ru,utf->trf/dot_general | solution.py:147
  118.8 12.4 %all_to_all.31 = bf16[16,128,128]{2,1,0:T(8,128)(2,1)S(1)} all-to-all(bf16[16,128,128]{2,1,0:T(8,128)(2,1)S(1)} %fusion.4), channel_id=1, replica_groups=mesh['ep'=32,'tp'=16] {'tp'}, dimensions={0} | all-to-all | bytes 1048576 | tf_op jit(solution)/shard_map/all_to_all | solution.py:148
  131.2 0.7 reduce_sum.108
  131.9 7.2 %all-to-all-start.4 = ((bf16[32,4,128]{2,1,0:T(4,128)(2,1)}), bf16[32,4,128]{2,1,0:T(4,128)(2,1)S(1)}, u32[]{:S(2)}, u32[]{:S(2)}) async-start(bf16[32,4,128]{2,1,0:T(4,128)(2,1)} %bitcast.23), calls=%async_computation.4 | async-start | bytes 65536 | tf_op jit(solution)/shard_map/all_to_all | solution.py:151
  139.1 0.1 select_reduce_fusion
  139.2 12.0 %all-to-all-done.4 = bf16[32,4,128]{2,1,0:T(4,128)(2,1)S(1)} async-done(((bf16[32,4,128]{2,1,0:T(4,128)(2,1)}), bf16[32,4,128]{2,1,0:T(4,128)(2,1)S(1)}, u32[]{:S(2)}, u32[]{:S(2)}) %all-to-all-start.4) | async-done | bytes 32800 | tf_op jit(solution)/shard_map/all_to_all | solution.py:151
  151.2 0.8 fusion.14
  152.0 9.2 %all_to_all.32 = bf16[16,16,128]{2,1,0:T(8,128)(2,1)S(1)} all-to-all(bf16[16,16,128]{2,1,0:T(8,128)(2,1)S(1)} %broadcast_in_dim.98), channel_id=1, replica_groups=mesh['ep'=32,'tp'=16] {'tp'}, dimensions={0} | all-to-all | bytes 131072 | tf_op jit(solution)/shard_map/all_to_all | solution.py:15
  161.2 0.6 copy_bitcast_fusion
  (31 shorter events, 0.3 us)
Async XLA Ops:
  0.0 60.1 %copy-start = (bf16[16,1,1024,64]{2,3,1,0:T(8,128)(2,1)S(1)}, bf16[16,1,1024,64]{2,3,1,0:T(8,128)(2,1)}, u32[]{:S(2)}) copy-start(bf16[16,1,1024,64]{2,3,1,0:T(8,128)(2,1)} %param.25) | copy-start | bytes 6291460
  0.0 47.2 %copy-start.5 = (bf16[2048]{0:T(1024)(128)(2,1)S(1)}, bf16[2048]{0:T(1024)(128)(2,1)}, u32[]{:S(2)}) copy-start(bf16[2048]{0:T(1024)(128)(2,1)} %param.19) | copy-start | bytes 12292
  0.0 47.2 %copy-start.1 = (bf16[16,2048]{1,0:T(8,128)(2,1)S(1)}, bf16[16,2048]{1,0:T(8,128)(2,1)}, u32[]{:S(2)}) copy-start(bf16[16,2048]{1,0:T(8,128)(2,1)} %param.18) | copy-start | bytes 196612
  37.5 19.2 %collective-permute-start = (bf16[1024,257]{0,1:T(8,128)(2,1)}, bf16[1024,257]{0,1:T(8,128)(2,1)S(1)}, u32[]{:S(2)}, u32[]{:S(2)}) collective-permute-start(bf16[1024,257]{0,1:T(8,128)(2,1)} %copy.118), channel_id=1, source_target_pairs={{0,16},{16,0},{32,48},{48,32},{64,80},{80,64},{96,112},{112,96},{1... | collective-permute-start | bytes 1579016 | tf_op jit(solution)/shard_map/ppermute | solution.py:53
  59.4 1.3 copy-start.2
  59.4 1.3 copy-start.7
  63.8 41.2 %copy-start.3 = (bf16[1,2048,64]{1,2,0:T(8,128)(2,1)S(1)}, bf16[1,2048,64]{1,2,0:T(8,128)(2,1)}, u32[]{:S(2)}) copy-start(bf16[1,2048,64]{1,2,0:T(8,128)(2,1)} %param.33) | copy-start | bytes 786436
  63.8 42.0 %copy-start.4 = (bf16[1,2048,64]{1,2,0:T(8,128)(2,1)S(1)}, bf16[1,2048,64]{1,2,0:T(8,128)(2,1)}, u32[]{:S(2)}) copy-start(bf16[1,2048,64]{1,2,0:T(8,128)(2,1)} %param.34) | copy-start | bytes 786436
  64.7 13.9 %all-to-all-start = ((f32[16,16,128]{2,1,0:T(8,128)}), f32[16,16,128]{2,1,0:T(8,128)S(1)}, u32[]{:S(2)}, u32[]{:S(2)}) async-start(f32[16,16,128]{2,1,0:T(8,128)} %convolution_bitcast_fusion), calls=%async_computation | async-start | bytes 262144 | tf_op jit(solution)/shard_map/all_to_all | solution.py:98
  101.4 14.3 %all-to-all-start.2 = ((bf16[16,144,128]{2,1,0:T(8,128)(2,1)}), bf16[16,144,128]{2,1,0:T(8,128)(2,1)S(1)}, u32[]{:S(2)}, u32[]{:S(2)}) async-start(bf16[16,144,128]{2,1,0:T(8,128)(2,1)} %broadcast_in_dim.97), calls=%async_computation.2 | async-start | bytes 1179648 | tf_op jit(solution)/shard_map/all_to_all | solution.py:15
  115.8 23.4 %copy-start.6 = (f32[16,4]{0,1:T(4,128)S(1)}, f32[16,4]{0,1:T(4,128)}, u32[]{:S(2)}) copy-start(f32[16,4]{0,1:T(4,128)} %param.32) | copy-start | bytes 772
  131.9 19.3 %all-to-all-start.4 = ((bf16[32,4,128]{2,1,0:T(4,128)(2,1)}), bf16[32,4,128]{2,1,0:T(4,128)(2,1)S(1)}, u32[]{:S(2)}, u32[]{:S(2)}) async-start(bf16[32,4,128]{2,1,0:T(4,128)(2,1)} %bitcast.23), calls=%async_computation.4 | async-start | bytes 65536 | tf_op jit(solution)/shard_map/all_to_all | solution.py:151

commit v2 on v1

--- a/solution.py
+++ b/solution.py
@@ -1,6 +1,8 @@
 import jax
 import jax.numpy as jnp
 from jax import lax
+from jax.experimental import pallas as pl
+from jax.experimental.pallas import tpu as pltpu
 from jax.sharding import PartitionSpec as P
 
 NORM_EPSILON = 1e-06
@@ -15,6 +17,99 @@
     return lax.all_to_all(
         jnp.broadcast_to(shard[None], (size, *shard.shape)), axis, 0, 0, tiled=True
     )
+
+
+PACK_ROWS = 72
+
+
+def attention_kernel(
+    core_ref, lengths_ref, bias_ref, tokens_ref, gain_ref, mine_ref, theirs_ref, gates_ref, keys_hbm, values_hbm,
+    out_ref, keys_ref, values_ref, sems,
+):
+    rows, width = tokens_ref.shape
+    cached = keys_ref.shape[1]
+    head = keys_ref.shape[0] // rows
+    chips = mine_ref.shape[0]
+    key_copy = pltpu.make_async_copy(keys_hbm, keys_ref, sems.at[0])
+    value_copy = pltpu.make_async_copy(values_hbm, values_ref, sems.at[1])
+    key_copy.start()
+    value_copy.start()
+
+    wide = tokens_ref[...].astype(F32)
+    scale_row = lax.rsqrt(jnp.mean(wide * wide, axis=-1, keepdims=True) + NORM_EPSILON)
+    normed = (wide * scale_row * gain_ref[...].astype(F32)).astype(BF16)
+
+    is_odd = core_ref[0] == 1
+    projected = jnp.zeros((rows, 256), F32)
+    shifted = jnp.zeros((rows, 128), F32)
+    forget = jnp.zeros((rows, 128), F32)
+    out_tiles = []
+    for z in range(chips):
+        own = mine_ref[z]
+        other = theirs_ref[z]
+        first = jnp.where(is_odd, other, own)
+        second = jnp.where(is_odd, own, other)
+        left = normed[:, z * 128 : (z + 1) * 128]
+        stacked = jnp.concatenate([first[:64, :128], second[:64, :128]], axis=0)
+        projected_qk = jnp.dot(left, stacked, preferred_element_type=F32)
+        both = jnp.concatenate([first[:64, 128:], second[:64, 128:]], axis=0)
+        lane = lax.broadcasted_iota(jnp.int32, left.shape, 1)
+        even_left = jnp.where(lane < 64, left, jnp.zeros_like(left))
+        odd_left = jnp.where(lane < 64, jnp.zeros_like(left), left)
+        projected = projected + jnp.concatenate(
+            [projected_qk, jnp.dot(odd_left, both, preferred_element_type=F32)], axis=1
+        )
+        shifted = shifted + jnp.dot(even_left, both, preferred_element_type=F32)
+        out_tiles.append((first[:64, 128:], second[:64, 128:]))
+        weights = jnp.concatenate([first[64:65, :64], second[64:65, :64]], axis=1)
+        forget = forget + left.astype(F32) * weights.astype(F32)
+    query = projected[:, :head].astype(BF16)
+    key_new = projected[:, head : 2 * head].astype(BF16)
+    value_new = (projected[:, 2 * head : 3 * head] + shifted[:, head:]).astype(BF16)
+    forget_pre = jnp.sum(forget, axis=1, keepdims=True) + bias_ref[0]
+    log_gate = jnp.minimum(forget_pre, 0.0) - jnp.log1p(jnp.exp(-jnp.abs(forget_pre)))
+
+    gates = gates_ref[...].reshape(rows, cached)
+    row = lax.broadcasted_iota(jnp.int32, (rows, 1), 0)
+    count = jnp.zeros((rows, 1), jnp.int32)
+    for s in range(rows):
+        count = jnp.where(row == s, lengths_ref[s], count)
+    position = lax.broadcasted_iota(jnp.int32, (rows, cached), 1)
+    last_gate = jnp.sum(jnp.where(position == count - 1, gates, 0.0), axis=-1, keepdims=True)
+    new_gate = last_gate + log_gate
+
+    owner = lax.broadcasted_iota(jnp.int32, (rows, rows * head), 1) // head
+    diagonal = owner == lax.broadcasted_iota(jnp.int32, (rows, rows * head), 0)
+    repeated = jnp.concatenate([query] * rows, axis=1)
+    spread = jnp.where(diagonal, repeated, jnp.zeros_like(repeated))
+    scale = head ** (-0.5)
+    key_copy.wait()
+    scores = jnp.dot(spread, keys_ref[...], preferred_element_type=F32) * scale
+    scores = scores + (new_gate - gates)
+    scores = jnp.where(position < count, scores, -jnp.inf)
+    own_score = jnp.sum(query.astype(F32) * key_new.astype(F32), axis=-1, keepdims=True) * scale
+    highest = jnp.maximum(jnp.max(scores, axis=-1, keepdims=True), own_score)
+    cached_weight = jnp.exp(scores - highest)
+    own_weight = jnp.exp(own_score - highest)
+    denominator = jnp.sum(cached_weight, axis=-1, keepdims=True) + own_weight
+    share = (cached_weight / denominator).astype(BF16)
+    value_copy.wait()
+    crossed = lax.dot_general(
+        share, values_ref[...], (((1,), (1,)), ((), ())), preferred_element_type=F32
+    )
+    crossed = jnp.where(diagonal, crossed, 0.0)
+    folded = crossed[:, :128]
+    for b in range(1, rows * head // 128):
+        folded = folded + crossed[:, b * 128 : (b + 1) * 128]
+    attended = folded[:, :head] + folded[:, head:]
+    attended = attended + (own_weight / denominator) * value_new.astype(F32)
+    attended = attended.astype(BF16)
+    lane = lax.broadcasted_iota(jnp.int32, (rows, 128), 1)
+    for z in range(chips):
+        first, second = out_tiles[z]
+        low = jnp.dot(attended, first, preferred_element_type=F32)
+        high = jnp.dot(attended, second, preferred_element_type=F32)
+        out_ref[z] = jnp.where(lane < head, low, high)
 
 
 def local(
@@ -47,54 +142,43 @@
     core = lax.axis_index("ep") % 2
     offset = lax.axis_index("tp") * narrow
 
-    packed = jnp.concatenate([w_query, w_key, w_value, w_out.T, w_forget], axis=1)
+    is_odd = core == 1
+    packed = jnp.concatenate(
+        [w_query, w_key, jnp.where(is_odd, w_value, w_out), jnp.where(is_odd, w_out, w_value)], axis=1
+    )
+    extra = jnp.pad(w_forget.T, ((0, PACK_ROWS - block - 1), (0, packed.shape[1] - block)))
+    packed = jnp.concatenate([packed, extra], axis=0)
     same_core = [[2 * z + c for z in range(chips)] for c in range(2)]
-    mine = lax.all_gather(packed, "ep", axis=0, tiled=True, axis_index_groups=same_core)
+    mine = lax.all_gather(packed, "ep", axis=0, tiled=False, axis_index_groups=same_core)
     theirs = lax.ppermute(mine, "ep", [(i, i ^ 1) for i in range(n_ep)])
 
-    wide = tokens.astype(F32)
-    normed = wide * lax.rsqrt(jnp.mean(wide * wide, axis=-1, keepdims=True) + NORM_EPSILON)
-    normed = (normed * attn_gain.astype(F32)).astype(BF16)
-    by_core = normed.reshape(rows, chips, 2, block)
-    even = by_core[:, :, 0].reshape(rows, chips * block)
-    odd = by_core[:, :, 1].reshape(rows, chips * block)
-    is_odd = core == 1
-    first = jnp.where(is_odd, theirs, mine)
-    second = jnp.where(is_odd, mine, theirs)
-    projected = jnp.dot(even, first, preferred_element_type=F32) + jnp.dot(
-        odd, second, preferred_element_type=F32
-    )
-    query = projected[:, :head].astype(BF16)
-    key_new = projected[:, head : 2 * head].astype(BF16)
-    value_new = projected[:, 2 * head : 3 * head].astype(BF16)
-    log_gate = jax.nn.log_sigmoid(projected[:, 4 * head] + forget_bias[0])
-
-    keys = cache_keys[:, 0]
-    values = cache_values[:, 0]
-    gates = cache_gates[:, 0]
-    scale = head ** (-0.5)
-    positions = jnp.arange(keys.shape[1], dtype=jnp.int32)
-    valid = positions[None, :] < lengths[:, None]
-    is_last = positions[None, :] == lengths[:, None] - 1
-    last_gate = jnp.sum(jnp.where(is_last, gates, F32(0.0)), axis=-1)
-    new_gate = last_gate + log_gate
-    scores = jnp.einsum("sd,sld->sl", query, keys, preferred_element_type=F32) * scale
-    scores = scores + (new_gate[:, None] - gates)
-    scores = jnp.where(valid, scores, -jnp.inf)
-    own_score = jnp.sum(query.astype(F32) * key_new.astype(F32), axis=-1) * scale
-    highest = jnp.maximum(jnp.max(scores, axis=-1), own_score)
-    cached_weight = jnp.exp(scores - highest[:, None])
-    own_weight = jnp.exp(own_score - highest)
-    denominator = jnp.sum(cached_weight, axis=-1) + own_weight
-    share = (cached_weight / denominator[:, None]).astype(BF16)
-    attended = jnp.einsum("sl,sld->sd", share, values, preferred_element_type=F32)
-    attended = attended + (own_weight / denominator)[:, None] * value_new.astype(F32)
-    attended = attended.astype(BF16)
-
-    out_first = first[:, 3 * head : 4 * head].reshape(chips, block, head)
-    out_second = second[:, 3 * head : 4 * head].reshape(chips, block, head)
-    out_blocks = jnp.concatenate([out_first, out_second], axis=1)
-    head_terms = jnp.einsum("sd,zfd->zsf", attended, out_blocks, preferred_element_type=F32)
+    cached = cache_keys.shape[2]
+    smem = pl.BlockSpec(memory_space=pltpu.SMEM)
+    vmem = pl.BlockSpec(memory_space=pltpu.VMEM)
+    anywhere = pl.BlockSpec(memory_space=pl.ANY)
+    head_terms = pl.pallas_call(
+        attention_kernel,
+        out_shape=jax.ShapeDtypeStruct((n_tp, rows, narrow), F32),
+        in_specs=[smem, smem, smem, vmem, vmem, vmem, vmem, vmem, anywhere, anywhere],
+        out_specs=vmem,
+        scratch_shapes=[
+            pltpu.VMEM((rows * head, cached), BF16),
+            pltpu.VMEM((rows * head, cached), BF16),
+            pltpu.SemaphoreType.DMA((2,)),
+        ],
+        name="attention",
+    )(
+        core.reshape(1),
+        lengths,
+        forget_bias,
+        tokens,
+        attn_gain.reshape(1, width),
+        mine,
+        theirs,
+        cache_gates,
+        jnp.swapaxes(cache_keys[:, 0], 1, 2).reshape(rows * head, cached),
+        jnp.swapaxes(cache_values[:, 0], 1, 2).reshape(rows * head, cached),
+    )
     parts = lax.all_to_all(head_terms, "tp", 0, 0, tiled=True)
     residual = lax.dynamic_slice_in_dim(tokens, offset, narrow, 1).astype(F32) + jnp.sum(parts, axis=0)
 

time: 163 us -> 150 us (0.920)
  local copies, waits for them, and re-layouts: 15 us -> 4.94 us
  matrix products: 8 us -> 2.16 us
  Pallas kernels: 0 us -> 5.42 us
  other arithmetic: 8.14 us -> 5.07 us
  waiting for transfers between devices: 26.5 us -> 28.8 us
  blocking collectives: 76 us -> 74.1 us
    pallas_call x0 -> x1, Pallas kernels: none -> 5.42 us  [local(): pl.pallas_call(attention_kernel, out_shape=jax.ShapeDtypeStruct((n_tp, ro...]
    dot_general x5 -> x0, matrix products: 3.93 us -> none  [the longest x1 2.23 us: local(): jnp.einsum('sl,sld->sd', share, values, preferred_element_type=F32)]
    unnamed x22 -> x16, local copies, waits for them, and re-layouts: 4.98 us -> 1.7 us
    all_to_all x1, waiting for transfers between devices: 8.26 us -> 10.6 us  [to_everyone(): lax.all_to_all(jnp.broadcast_to(shard[None], (size, *shard.shape)), axis,...]
    another operation x2 -> x0, local copies, waits for them, and re-layouts: 1.9 us -> none  [the longest x1 0.95 us: local(): even = by_core[:, :, 0].reshape(rows, chips * block)]
    all_gather x1, blocking collectives: 33.9 us -> 32.1 us  [local(): lax.all_gather(packed, 'ep', axis=0, tiled=False, axis_index_groups=same_...]
    slice x4 -> x0, local copies, waits for them, and re-layouts: 1.66 us -> none  [the longest x1 1.39 us: local(): even = by_core[:, :, 0].reshape(rows, chips * block)]
  transfers between devices with their start and end apart: 4 -> 4, of which waited for: 3 -> 3; matrix products, arithmetic and copies ran while one was open for 8% -> 3% of each run, Pallas kernels for 0% -> 0%
where the time goes in v2:
time: 150 us; the launch traced here: 149 us
  blocking collectives  74.1 us (49%)
  waiting for transfers between devices  28.8 us (19%)
  starting transfers between devices  27.8 us (19%)
  Pallas kernels  5.42 us (4%)
  other arithmetic  5.07 us (3%)
  local copies, waits for them, and re-layouts  4.94 us (3%)
  matrix products  2.16 us (1%)
    all_gather x1, blocking collectives, local(): lax.all_gather(packed, 'ep', axis=0, tiled=False, axis_index_groups=same_...  32.1 us
    all_to_all x1, blocking collectives, local(): received = lax.all_to_all(sent, 'ep', 0, 0, tiled=True)  20.4 us
    all_to_all x1, blocking collectives, local(): partial = lax.all_to_all(partial, 'tp', 0, 0, tiled=True)  12.4 us
    all_to_all x1, waiting for transfers between devices, local(): lax.all_to_all(served.reshape(n_ep, capacity, narrow), 'ep', 0, 0, tiled=...  12 us
    all_to_all x1, waiting for transfers between devices, to_everyone(): lax.all_to_all(jnp.broadcast_to(shard[None], (size, *shard.shape)), axis,...  10.6 us
    ppermute x1, starting transfers between devices, local(): theirs = lax.ppermute(mine, 'ep', [(i, i ^ 1) for i in range(n_ep)])  10.1 us
    all_to_all x1, blocking collectives, to_everyone(): lax.all_to_all(jnp.broadcast_to(shard[None], (size, *shard.shape)), axis,...  9.19 us
    all_to_all x1, starting transfers between devices, local(): lax.all_to_all(served.reshape(n_ep, capacity, narrow), 'ep', 0, 0, tiled=...  7.23 us
  transfers between devices with their start and end apart: 4, of which 3 were waited for; matrix products, arithmetic and copies ran while one was open for 3% of the time, Pallas kernels for 0%

profile of v2, /device:TPU:1, one launch (start us, length us, event | category | flops | bytes accessed | tf_op | source)
XLA Modules:
  0.0 149.2 jit_solution(5751801986634077708)
XLA Ops:
  0.0 0.7 broadcast_select_fusion.1
  0.7 0.8 fusion.21
  1.6 32.1 %all-gather = bf16[1152,256]{1,0:T(8,128)(2,1)S(1)} all-gather(bf16[72,256]{1,0:T(8,128)(2,1)S(1)} %fusion.21), channel_id=2, replica_groups={{0,32,64,96,128,160,192,224,256,288,320,352,384,416,448,480},{16,48,80,..., dimensions={0}, use_global_device_ids=true | all-gather | bytes 626688 | tf_op jit(solution)/shard_map/all_gather | solution.py:152
  33.7 0.0 copy-start
  33.7 10.1 %collective-permute-start = (bf16[16,72,256]{2,1,0:T(8,128)(2,1)S(1)}, bf16[16,72,256]{2,1,0:T(8,128)(2,1)S(1)}, u32[]{:S(2)}, u32[]{:S(2)}) collective-permute-start(bf16[16,72,256]{2,1,0:T(8,128)(2,1)S(1)} %bitcast.72), channel_id=1, source_target_pairs={{0,16},{16,0},{32,48},{48,32},{64,80},{80,64},{96,112},{112,96},{1... | collective-permute-start | bytes 1769480 | tf_op jit(solution)/shard_map/ppermute | solution.py:153
  43.9 1.3 reshape.70.gain_ref
  45.8 0.8 copy.54
  46.6 0.1 eq.57
  46.7 0.2 convert_reduce_fusion
  46.8 0.1 reduce_sum.61
  46.9 0.1 copy.55
  47.0 0.7 multiply_add_fusion
  47.7 0.0 collective-permute-done.theirs_ref
  47.7 0.0 copy-start.1
  47.7 0.0 copy-done
  47.7 0.8 copy-done.1
  48.5 5.4 %attention.1 = f32[16,16,128]{2,1,0:T(8,128)} custom-call(s32[1]{0:T(128)} %bitcast.core_ref, s32[16]{0:T(128)} %lengths_ref.1, f32[1]{0:T(128)S(6)} %copy.73.bias_ref, bf16[16,2048]{1,0:T(8,128)(2,1)} %tokens_ref.1, bf16[1,2048]{1,0:T(2,128)(2,1)} %reshape.70.gain_ref, bf16[16,72,256]{2,1,0:T(8,128)(2,1)} %bitcast.73, bf16[16,72,256]{2,1,0:T(8,128)(2,1)} %copy-done.1, ...), custom_call_target="tpu_custom_call" | custom-call | tf_op jit(solution)/shard_map/attention/pallas_call | solution.py:159
  54.0 0.0 copy-start.2
  54.0 0.0 copy-start.3
  54.0 0.0 copy-start.4
  54.0 6.9 %all-to-all-start = ((f32[16,16,128]{2,1,0:T(8,128)}), f32[16,16,128]{2,1,0:T(8,128)S(1)}, u32[]{:S(2)}, u32[]{:S(2)}) async-start(f32[16,16,128]{2,1,0:T(8,128)} %attention.1), calls=%async_computation | async-start | bytes 262144 | tf_op jit(solution)/shard_map/all_to_all | solution.py:182
  60.9 0.8 dynamic-slice_convert_fusion
  61.7 0.1 fusion.27
  61.7 6.3 %all-to-all-done = f32[16,16,128]{2,1,0:T(8,128)S(1)} async-done(((f32[16,16,128]{2,1,0:T(8,128)}), f32[16,16,128]{2,1,0:T(8,128)S(1)}, u32[]{:S(2)}, u32[]{:S(2)}) %all-to-all-start) | async-done | bytes 131104 | tf_op jit(solution)/shard_map/all_to_all | solution.py:182
  68.1 0.8 multiply_convert_fusion
  68.9 0.1 select_select_fusion
  69.0 0.2 convolution_convert_fusion.1
  69.2 20.4 %all_to_all.30 = bf16[32,8,128]{2,1,0:T(8,128)(2,1)S(1)} all-to-all(bf16[32,8,128]{2,1,0:T(8,128)(2,1)S(1)} %pad_maximum_fusion), channel_id=1, replica_groups=mesh['ep'=32,'tp'=16] {'ep'}, dimensions={0} | all-to-all | bytes 131072 | tf_op jit(solution)/shard_map/all_to_all | solution.py:212
  89.7 0.1 copy.56
  89.8 0.9 broadcast_in_dim.77
  90.7 3.6 %all-to-all-start.2 = ((bf16[16,144,128]{2,1,0:T(8,128)(2,1)}), bf16[16,144,128]{2,1,0:T(8,128)(2,1)S(1)}, u32[]{:S(2)}, u32[]{:S(2)}) async-start(bf16[16,144,128]{2,1,0:T(8,128)(2,1)} %broadcast_in_dim.77), calls=%async_computation.2 | async-start | bytes 1179648 | tf_op jit(solution)/shard_map/all_to_all | solution.py:17
  94.3 0.0 copy-done.2
  94.3 0.0 copy-done.3
  94.4 0.0 copy-done.4
  94.4 10.6 %all-to-all-done.2 = bf16[16,144,128]{2,1,0:T(8,128)(2,1)S(1)} async-done(((bf16[16,144,128]{2,1,0:T(8,128)(2,1)}), bf16[16,144,128]{2,1,0:T(8,128)(2,1)S(1)}, u32[]{:S(2)}, u32[]{:S(2)}) %all-to-all-start.2) | async-done | bytes 589856 | tf_op jit(solution)/shard_map/all_to_all | solution.py:17
  105.1 0.0 copy-start.5
  105.1 0.3 fusion.2
  105.4 0.8 fusion
  106.2 12.4 %all_to_all.31 = bf16[16,128,128]{2,1,0:T(8,128)(2,1)S(1)} all-to-all(bf16[16,128,128]{2,1,0:T(8,128)(2,1)S(1)} %fusion), channel_id=1, replica_groups=mesh['ep'=32,'tp'=16] {'tp'}, dimensions={0} | all-to-all | bytes 1048576 | tf_op jit(solution)/shard_map/all_to_all | solution.py:232
  118.6 0.7 reduce_sum.65
  119.3 7.2 %all-to-all-start.4 = ((bf16[32,4,128]{2,1,0:T(4,128)(2,1)}), bf16[32,4,128]{2,1,0:T(4,128)(2,1)S(1)}, u32[]{:S(2)}, u32[]{:S(2)}) async-start(bf16[32,4,128]{2,1,0:T(4,128)(2,1)} %bitcast.18), calls=%async_computation.4 | async-start | bytes 65536 | tf_op jit(solution)/shard_map/all_to_all | solution.py:235
  126.5 0.0 copy-done.5
  126.5 0.1 select_reduce_fusion
  126.6 12.0 %all-to-all-done.4 = bf16[32,4,128]{2,1,0:T(4,128)(2,1)S(1)} async-done(((bf16[32,4,128]{2,1,0:T(4,128)(2,1)}), bf16[32,4,128]{2,1,0:T(4,128)(2,1)S(1)}, u32[]{:S(2)}, u32[]{:S(2)}) %all-to-all-start.4) | async-done | bytes 32800 | tf_op jit(solution)/shard_map/all_to_all | solution.py:235
  138.6 0.8 fusion.10
  139.4 9.2 %all_to_all.32 = bf16[16,16,128]{2,1,0:T(8,128)(2,1)S(1)} all-to-all(bf16[16,16,128]{2,1,0:T(8,128)(2,1)S(1)} %broadcast_in_dim.78), channel_id=1, replica_groups=mesh['ep'=32,'tp'=16] {'tp'}, dimensions={0} | all-to-all | bytes 131072 | tf_op jit(solution)/shard_map/all_to_all | solution.py:17
  148.6 0.6 copy_bitcast_fusion
  (14 shorter events, 0.3 us)
Async XLA Ops:
  33.7 14.0 %copy-start = (bf16[1152,256]{1,0:T(8,128)(2,1)}, bf16[1152,256]{1,0:T(8,128)(2,1)S(1)}, u32[]{:S(2)}) copy-start(bf16[1152,256]{1,0:T(8,128)(2,1)S(1)} %all-gather) | copy-start | bytes 1769476
  33.7 14.0 %collective-permute-start = (bf16[16,72,256]{2,1,0:T(8,128)(2,1)S(1)}, bf16[16,72,256]{2,1,0:T(8,128)(2,1)S(1)}, u32[]{:S(2)}, u32[]{:S(2)}) collective-permute-start(bf16[16,72,256]{2,1,0:T(8,128)(2,1)S(1)} %bitcast.72), channel_id=1, source_target_pairs={{0,16},{16,0},{32,48},{48,32},{64,80},{80,64},{96,112},{112,96},{1... | collective-permute-start | bytes 1769480 | tf_op jit(solution)/shard_map/ppermute | solution.py:153
  47.7 0.8 copy-start.1
  54.0 40.3 %copy-start.2 = (bf16[1,2048,64]{1,2,0:T(8,128)(2,1)S(1)}, bf16[1,2048,64]{1,2,0:T(8,128)(2,1)}, u32[]{:S(2)}) copy-start(bf16[1,2048,64]{1,2,0:T(8,128)(2,1)} %param.33) | copy-start | bytes 786436
  54.0 40.4 %copy-start.3 = (bf16[1,2048,64]{1,2,0:T(8,128)(2,1)S(1)}, bf16[1,2048,64]{1,2,0:T(8,128)(2,1)}, u32[]{:S(2)}) copy-start(bf16[1,2048,64]{1,2,0:T(8,128)(2,1)} %param.34) | copy-start | bytes 786436
  54.0 40.4 %copy-start.4 = (bf16[1,64,2048]{2,1,0:T(8,128)(2,1)S(1)}, bf16[1,64,2048]{2,1,0:T(8,128)(2,1)}, u32[]{:S(2)}) copy-start(bf16[1,64,2048]{2,1,0:T(8,128)(2,1)} %param.35) | copy-start | bytes 786436
  54.0 14.0 %all-to-all-start = ((f32[16,16,128]{2,1,0:T(8,128)}), f32[16,16,128]{2,1,0:T(8,128)S(1)}, u32[]{:S(2)}, u32[]{:S(2)}) async-start(f32[16,16,128]{2,1,0:T(8,128)} %attention.1), calls=%async_computation | async-start | bytes 262144 | tf_op jit(solution)/shard_map/all_to_all | solution.py:182
  90.7 14.3 %all-to-all-start.2 = ((bf16[16,144,128]{2,1,0:T(8,128)(2,1)}), bf16[16,144,128]{2,1,0:T(8,128)(2,1)S(1)}, u32[]{:S(2)}, u32[]{:S(2)}) async-start(bf16[16,144,128]{2,1,0:T(8,128)(2,1)} %broadcast_in_dim.77), calls=%async_computation.2 | async-start | bytes 1179648 | tf_op jit(solution)/shard_map/all_to_all | solution.py:17
  105.1 21.5 %copy-start.5 = (f32[16,4]{0,1:T(4,128)S(1)}, f32[16,4]{0,1:T(4,128)}, u32[]{:S(2)}) copy-start(f32[16,4]{0,1:T(4,128)} %param.32) | copy-start | bytes 772
  119.3 19.3 %all-to-all-start.4 = ((bf16[32,4,128]{2,1,0:T(4,128)(2,1)}), bf16[32,4,128]{2,1,0:T(4,128)(2,1)S(1)}, u32[]{:S(2)}, u32[]{:S(2)}) async-start(bf16[32,4,128]{2,1,0:T(4,128)(2,1)} %bitcast.18), calls=%async_computation.4 | async-start | bytes 65536 | tf_op jit(solution)/shard_map/all_to_all | solution.py:235

commit v3 on v2

v3 whole, which is shorter than its diff:
```python
import jax
import jax.numpy as jnp
from jax import lax
from jax.experimental import pallas as pl
from jax.experimental.pallas import tpu as pltpu
from jax.sharding import PartitionSpec as P

NORM_EPSILON = 1e-06
CLAMP_LIMIT = 7.0
SIGMOID_SLOPE = 1.702
F32 = jnp.float32
BF16 = jnp.bfloat16


def to_everyone(shard, axis):
    size = lax.axis_size(axis)
    return lax.all_to_all(
        jnp.broadcast_to(shard[None], (size, *shard.shape)), axis, 0, 0, tiled=True
    )


PACK_ROWS = 72
LIMIT = 16 * 2**20
CAPACITY = 4


def settle_kernel(packed_ref, out_ref):
    out_ref[...] = packed_ref[...]


def prepare_kernel(
    core_ref, place_ref, mine_ref, tokens_ref, gain_ref, moe_gain_ref, routing_ref, weight_ref,
    normed_ref, sums_ref, slice_ref, moe_slice_ref, choice_ref, mix_ref,
):
    rows, width = tokens_ref.shape
    narrow = slice_ref.shape[1]
    tokens = tokens_ref[...]
    wide = tokens.astype(F32)
    scale_row = lax.rsqrt(jnp.mean(wide * wide, axis=-1, keepdims=True) + NORM_EPSILON)
    normed = (wide * scale_row * gain_ref[...].astype(F32).reshape(1, width)).astype(BF16)
    normed_ref[...] = normed
    sums_ref[...] = half_sums(normed, mine_ref, core_ref[0], rows)

    place = place_ref[0]
    moe_gain = moe_gain_ref[...].astype(F32).reshape(1, width)
    part = jnp.zeros((rows, narrow), F32)
    moe_part = jnp.zeros((1, narrow), F32)
    for t in range(width // narrow):
        part = jnp.where(place == t, wide[:, t * narrow : (t + 1) * narrow], part)
        moe_part = jnp.where(place == t, moe_gain[:, t * narrow : (t + 1) * narrow], moe_part)
    slice_ref[...] = part
    moe_slice_ref[...] = jnp.broadcast_to(moe_part, moe_slice_ref.shape)

    slots = choice_ref.shape[1]
    top = routing_ref.shape[0]
    capacity = CAPACITY
    i = lax.broadcasted_iota(jnp.int32, (rows, rows), 0)
    j = lax.broadcasted_iota(jnp.int32, (rows, rows), 1)
    eye = (i == j).astype(F32)
    across = (((1,), (1,)), ((), ()))
    chosen = lax.dot_general(
        eye, routing_ref[...].astype(F32), across, precision=lax.Precision.HIGHEST, preferred_element_type=F32
    )
    weights = lax.dot_general(
        eye, weight_ref[...], across, precision=lax.Precision.HIGHEST, preferred_element_type=F32
    )
    lane = lax.broadcasted_iota(jnp.int32, (rows, slots), 1)
    expert = (lane // capacity).astype(F32)
    named = jnp.zeros((rows, slots), F32)
    weight = jnp.zeros((rows, slots), F32)
    for k in range(top):
        hit = chosen[:, k : k + 1] == expert
        named = jnp.where(hit, 1.0, named)
        weight = jnp.where(hit, weights[:, k : k + 1], weight)
    earlier = jnp.dot((j < i).astype(BF16), named.astype(BF16), preferred_element_type=F32)
    filled = (named > 0.5) & (earlier == (lane % capacity).astype(F32))
    choice_ref[...] = jnp.where(filled, 1.0, 0.0).astype(BF16)
    mix_ref[...] = jnp.where(filled, weight, 0.0)


def half_sums(normed, packed_ref, core, rows):
    lane = lax.broadcasted_iota(jnp.int32, (rows, 128), 1)
    taken = (lane // 64) == core
    total = jnp.zeros((rows, 256), F32)
    forget = jnp.zeros((rows, 128), F32)
    for z in range(packed_ref.shape[0]):
        left = normed[:, z * 128 : (z + 1) * 128]
        left = jnp.where(taken, left, jnp.zeros_like(left))
        block = packed_ref[z, :64, :]
        total = total + jnp.dot(left, jnp.concatenate([block, block], axis=0), preferred_element_type=F32)
        weights = packed_ref[z, 64:72, :128][:1, :64]
        forget = forget + left.astype(F32) * jnp.concatenate([weights, weights], axis=1).astype(F32)
    return jnp.concatenate([total, forget], axis=1)


def attention_kernel(
    core_ref, bias_ref, lengths_ref, normed_ref, sums_ref, mine_ref, theirs_ref, keys_ref, values_ref, gates_ref, out_ref
):
    rows = normed_ref.shape[0]
    cached = keys_ref.shape[1]
    head = keys_ref.shape[0] // rows
    chips = mine_ref.shape[0]
    core = core_ref[0]
    is_odd = core == 1
    own = sums_ref[...]
    other = half_sums(normed_ref[...], theirs_ref, 1 - core, rows)
    both = own + other
    query = both[:, :head].astype(BF16)
    key_new = both[:, head : 2 * head].astype(BF16)
    value_new = both[:, 2 * head : 3 * head].astype(BF16)
    forget_pre = jnp.sum(both[:, 256:], axis=1, keepdims=True) + bias_ref[0]
    log_gate = jnp.minimum(forget_pre, 0.0) - jnp.log1p(jnp.exp(-jnp.abs(forget_pre)))

    gates = gates_ref[...].reshape(rows, cached)
    row = lax.broadcasted_iota(jnp.int32, (rows, 1), 0)
    count = jnp.zeros((rows, 1), jnp.int32)
    for s in range(rows):
        count = jnp.where(row == s, lengths_ref[s], count)
    position = lax.broadcasted_iota(jnp.int32, (rows, cached), 1)
    last_gate = jnp.sum(jnp.where(position == count - 1, gates, 0.0), axis=-1, keepdims=True)
    new_gate = last_gate + log_gate

    owner = lax.broadcasted_iota(jnp.int32, (rows, rows * head), 1) // head
    diagonal = owner == lax.broadcasted_iota(jnp.int32, (rows, rows * head), 0)
    repeated = jnp.concatenate([query] * rows, axis=1)
    spread = jnp.where(diagonal, repeated, jnp.zeros_like(repeated))
    scale = head ** (-0.5)
    scores = jnp.dot(spread, keys_ref[...], preferred_element_type=F32) * scale
    scores = scores + (new_gate - gates)
    scores = jnp.where(position < count, scores, -jnp.inf)
    own_score = jnp.sum(query.astype(F32) * key_new.astype(F32), axis=-1, keepdims=True) * scale
    highest = jnp.maximum(jnp.max(scores, axis=-1, keepdims=True), own_score)
    cached_weight = jnp.exp(scores - highest)
    own_weight = jnp.exp(own_score - highest)
    denominator = jnp.sum(cached_weight, axis=-1, keepdims=True) + own_weight
    share = (cached_weight / denominator).astype(BF16)
    crossed = lax.dot_general(
        share, values_ref[...], (((1,), (1,)), ((), ())), preferred_element_type=F32
    )
    crossed = jnp.where(diagonal, crossed, 0.0)
    folded = crossed[:, :128]
    for b in range(1, rows * head // 128):
        folded = folded + crossed[:, b * 128 : (b + 1) * 128]
    attended = folded[:, :head] + folded[:, head:]
    attended = attended + (own_weight / denominator) * value_new.astype(F32)
    attended = attended.astype(BF16)
    lane = lax.broadcasted_iota(jnp.int32, (rows, 128), 1)
    for z in range(chips):
        mine = jnp.dot(attended, mine_ref[z, :64, 128:], preferred_element_type=F32)
        theirs = jnp.dot(attended, theirs_ref[z, :64, 128:], preferred_element_type=F32)
        even = jnp.where(is_odd, theirs, mine)
        odd = jnp.where(is_odd, mine, theirs)
        out_ref[z] = jnp.where(lane < head, pltpu.roll(even, head, 1), odd)


def expert_kernel(rows_ref, gain_ref, gate_ref, up_ref, down_ref, out_ref):
    tiles, slots, narrow = rows_ref.shape
    width = tiles * narrow
    inverse = 1.0 / gain_ref[...].astype(F32).reshape(1, width)
    squares = jnp.zeros((slots, narrow), F32)
    products = jnp.zeros((slots, 2 * gate_ref.shape[0]), F32)
    for t in range(tiles):
        part = rows_ref[t]
        plain = part.astype(F32) * inverse[:, t * narrow : (t + 1) * narrow]
        squares = squares + plain * plain
        weights = jnp.concatenate(
            [gate_ref[:, t * narrow : (t + 1) * narrow], up_ref[:, t * narrow : (t + 1) * narrow]], axis=0
        )
        products = products + lax.dot_general(
            part, weights, (((1,), (1,)), ((), ())), preferred_element_type=F32
        )
    row_scale = lax.rsqrt(jnp.sum(squares, axis=1, keepdims=True) / width + NORM_EPSILON)
    products = products * row_scale
    units = gate_ref.shape[0]
    gate_cut = jnp.minimum(products[:, :units], CLAMP_LIMIT)
    up_cut = jnp.clip(products[:, units:], -CLAMP_LIMIT, CLAMP_LIMIT)
    hidden = ((up_cut + 1.0) * gate_cut * jax.nn.sigmoid(SIGMOID_SLOPE * gate_cut)).astype(BF16)
    for t in range(tiles):
        part = jnp.dot(hidden, down_ref[:, t * narrow : (t + 1) * narrow], preferred_element_type=F32)
        out_ref[t] = part.astype(BF16)


def spread_kernel(parts_ref, slice_ref, moe_slice_ref, choice_ref, residual_ref, sent_ref):
    residual = slice_ref[...]
    for t in range(parts_ref.shape[0]):
        residual = residual + parts_ref[t]
    residual_ref[...] = residual
    scaled = (residual * moe_slice_ref[:1, :]).astype(BF16)
    sent_ref[...] = lax.dot_general(
        choice_ref[...], scaled, (((0,), (0,)), ((), ())), preferred_element_type=F32
    ).astype(BF16)


def gather_kernel(parts_ref, out_ref):
    total = parts_ref[0].astype(F32)
    for t in range(1, parts_ref.shape[0]):
        total = total + parts_ref[t].astype(F32)
    out_ref[...] = total.astype(BF16)


def combine_kernel(returned_ref, mix_ref, residual_ref, out_ref):
    expert_sum = jnp.dot(
        mix_ref[...],
        returned_ref[...].astype(F32),
        precision=lax.Precision.HIGHEST,
        preferred_element_type=F32,
    )
    out = (residual_ref[...] + expert_sum).astype(BF16)
    for t in range(out_ref.shape[0]):
        out_ref[t] = out


def local(
    tokens,
    attn_gain,
    w_query,
    w_key,
    w_value,
    w_forget,
    forget_bias,
    cache_keys,
    cache_values,
    cache_gates,
    lengths,
    w_out,
    moe_gain,
    routing,
    route_weight,
    w_gate,
    w_up,
    w_down,
):
    n_ep = lax.axis_size("ep")
    n_tp = lax.axis_size("tp")
    rows, width = tokens.shape
    narrow = width // n_tp
    chips = n_ep // 2
    head = cache_keys.shape[3]
    cached = cache_keys.shape[2]
    slots = n_ep * CAPACITY
    core = (lax.axis_index("ep") % 2).reshape(1)
    place = lax.axis_index("tp").reshape(1)
    smem = pl.BlockSpec(memory_space=pltpu.SMEM)
    vmem = pl.BlockSpec(memory_space=pltpu.VMEM)
    params = pltpu.CompilerParams(vmem_limit_bytes=LIMIT)

    busy = pl.CostEstimate(flops=10**9, bytes_accessed=1, transcendentals=0)

    def kernel(body, name, outs, ins, cost=None):
        return pl.pallas_call(
            body,
            out_shape=tuple(jax.ShapeDtypeStruct(*o) for o in outs),
            in_specs=ins,
            out_specs=tuple(vmem for _ in outs),
            compiler_params=params,
            cost_estimate=cost,
            name=name,
        )

    packed = jnp.concatenate([w_query, w_key, w_value, w_out], axis=1)
    forget_row = jnp.pad(w_forget.T, ((0, PACK_ROWS - 65), (0, packed.shape[1] - 64)))
    packed = jnp.concatenate([packed, forget_row], axis=0)
    (packed,) = kernel(settle_kernel, "settle", [(packed.shape, BF16)], [vmem], cost=busy)(packed)
    same_core = [[2 * z + c for z in range(chips)] for c in range(2)]
    mine = lax.all_gather(packed, "ep", axis=0, tiled=False, axis_index_groups=same_core)
    theirs = lax.ppermute(mine, "ep", [(i, i ^ 1) for i in range(n_ep)])

    normed, sums, token_slice, moe_slice, choice, mix = kernel(
        prepare_kernel,
        "prepare",
        [
            ((rows, width), BF16),
            ((rows, 384), F32),
            ((rows, narrow), F32),
            ((8, narrow), F32),
            ((rows, slots), BF16),
            ((rows, slots), F32),
        ],
        [smem, smem] + [vmem] * 6,
        cost=busy,
    )(
        core,
        place,
        mine,
        tokens,
        attn_gain,
        moe_gain,
        routing.T,
        route_weight.T,
    )
    (head_terms,) = kernel(
        attention_kernel,
        "attention",
        [((n_tp, rows, narrow), F32)],
        [smem, smem, smem] + [vmem] * 7,
        cost=busy,
    )(
        core,
        forget_bias,
        lengths,
        normed,
        sums,
        mine,
        theirs,
        jnp.swapaxes(cache_keys[:, 0], 1, 2).reshape(rows * head, cached),
        jnp.swapaxes(cache_values[:, 0], 1, 2).reshape(rows * head, cached),
        cache_gates,
    )

    parts = lax.all_to_all(head_terms, "tp", 0, 0, tiled=True)
    residual, sent = kernel(
        spread_kernel, "spread", [((rows, narrow), F32), ((slots, narrow), BF16)], [vmem] * 4
    )(parts, token_slice, moe_slice, choice)
    received = lax.all_to_all(sent.reshape(n_ep, CAPACITY, narrow), "ep", 0, 0, tiled=True)
    full = to_everyone(received.reshape(slots, narrow), "tp")
    (partial,) = kernel(expert_kernel, "experts", [((n_tp, slots, narrow), BF16)], [vmem] * 5)(
        full, moe_gain, jnp.swapaxes(w_gate[0], 0, 1), jnp.swapaxes(w_up[0], 0, 1), w_down[0]
    )
    partial = lax.all_to_all(partial, "tp", 0, 0, tiled=True)
    (served,) = kernel(gather_kernel, "served", [((slots, narrow), BF16)], [vmem])(partial)
    returned = lax.all_to_all(served.reshape(n_ep, CAPACITY, narrow), "ep", 0, 0, tiled=True)
    (copies_out,) = kernel(combine_kernel, "combine", [((n_tp, rows, narrow), BF16)], [vmem] * 3)(
        returned.reshape(slots, narrow), mix, residual
    )
    final = lax.all_to_all(copies_out, "tp", 0, 0, tiled=True)
    return jnp.moveaxis(final, 0, 1).reshape(rows, width)


def solution(mesh):
    in_specs = (
        P("ep", None),
        P(),
        P("ep", "tp"),
        P("ep", "tp"),
        P("ep", "tp"),
        P("ep", "tp"),
        P("tp"),
        P("ep", "tp", None, None),
        P("ep", "tp", None, None),
        P("ep", "tp", None),
        P("ep"),
        P("tp", "ep"),
        P(),
        P("ep", None),
        P("ep", None),
        P("ep", None, "tp"),
        P("ep", None, "tp"),
        P("ep", "tp", None),
    )
    out_specs = P("ep", None)
    return jax.shard_map(local, mesh=mesh, in_specs=in_specs, out_specs=out_specs, check_vma=False)
```

time: 150 us -> 138 us (0.920)
  blocking collectives: 74.1 us -> 119 us
  waiting for transfers between devices: 28.8 us -> 0.31 us
  starting transfers between devices: 27.8 us -> 10.1 us
  other arithmetic: 5.07 us -> 0.87 us
  local copies, waits for them, and re-layouts: 4.94 us -> 1.44 us
  matrix products: 2.16 us -> 0 us
    all_to_all x1 -> x4, blocking collectives: 20.4 us -> 60.8 us  [the longest x1 19.4 us: local(): lax.all_to_all(sent.reshape(n_ep, CAPACITY, narrow), 'ep', 0, 0, tiled=True)]
    all_to_all x3 -> x0, waiting for transfers between devices: 28.8 us -> none  [the longest x1 12 us: local(): lax.all_to_all(served.reshape(n_ep, capacity, narrow), 'ep', 0, 0, tiled=...]
    all_to_all x3 -> x0, starting transfers between devices: 17.7 us -> none  [the longest x1 7.23 us: local(): lax.all_to_all(served.reshape(n_ep, capacity, narrow), 'ep', 0, 0, tiled=...]
    all_to_all x1, blocking collectives: 9.19 us -> 13 us  [to_everyone(): lax.all_to_all(jnp.broadcast_to(shard[None], (size, *shard.shape)), axis,...]
    dot_general x4 -> x0, matrix products: 2.16 us -> none  [the longest x1 0.84 us: local(): jnp.einsum('ru,utf->trf', hidden, down, preferred_element_type=F32)]
    convert_element_type x3 -> x0, other arithmetic: 1.58 us -> none  [the longest x1 0.81 us: local(): scaled = (residual * gain_here).astype(BF16)]
    pallas_call x1 -> x7, Pallas kernels: 5.42 us -> 4.75 us  [the longest x1 2.64 us: local(): kernel(attention_kernel, 'attention', [((n_tp, rows, narrow), F32)], [sme...]
  transfers between devices with their start and end apart: 4 -> 1, of which waited for: 3 -> 1; matrix products, arithmetic and copies ran while one was open for 3% -> 0% of each run, Pallas kernels for 0% -> 0%
where the time goes in v3:
time: 138 us; the launch traced here: 137 us
  blocking collectives  119 us (86%)
  starting transfers between devices  10.1 us (7%)
  Pallas kernels  4.75 us (3%)
  local copies, waits for them, and re-layouts  1.44 us (1%)
    all_gather x1, blocking collectives, local(): lax.all_gather(packed, 'ep', axis=0, tiled=False, axis_index_groups=same_...  32.3 us
    all_to_all x1, blocking collectives, local(): lax.all_to_all(sent.reshape(n_ep, CAPACITY, narrow), 'ep', 0, 0, tiled=True)  19.4 us
    all_to_all x1, blocking collectives, local(): lax.all_to_all(served.reshape(n_ep, CAPACITY, narrow), 'ep', 0, 0, tiled=...  18.4 us
    all_to_all x1, blocking collectives, local(): parts = lax.all_to_all(head_terms, 'tp', 0, 0, tiled=True)  13.8 us
    all_to_all x1, blocking collectives, to_everyone(): lax.all_to_all(jnp.broadcast_to(shard[None], (size, *shard.shape)), axis,...  13 us
    all_to_all x1, blocking collectives, local(): partial = lax.all_to_all(partial, 'tp', 0, 0, tiled=True)  12.4 us
    ppermute x1, starting transfers between devices, local(): theirs = lax.ppermute(mine, 'ep', [(i, i ^ 1) for i in range(n_ep)])  10.1 us
    all_to_all x1, blocking collectives, local(): final = lax.all_to_all(copies_out, 'tp', 0, 0, tiled=True)  9.19 us
  transfers between devices with their start and end apart: 1, of which 1 were waited for; matrix products, arithmetic and copies ran while one was open for 0% of the time, Pallas kernels for 0%

profile of v3, /device:TPU:1, one launch (start us, length us, event | category | flops | bytes accessed | tf_op | source)
XLA Modules:
  0.0 136.9 jit_solution(4971923008957106685)
XLA Ops:
  0.0 0.9 fusion.1.packed_ref
  0.9 0.0 copy-start.6
  0.9 0.0 copy-start.8
  0.9 0.0 copy-start.9
  0.9 0.0 copy-start.10
  0.9 0.0 copy-start.11
  0.9 0.0 copy-start
  1.0 0.0 copy-start.5
  1.0 0.0 copy-start.7
  1.0 32.3 %all-gather = bf16[1152,256]{1,0:T(8,128)(2,1)S(1)} all-gather(bf16[72,256]{1,0:T(8,128)(2,1)S(1)} %settle.1), channel_id=2, replica_groups={{0,32,64,96,128,160,192,224,256,288,320,352,384,416,448,480},{16,48,80,..., dimensions={0}, use_global_device_ids=true | all-gather | bytes 626688 | tf_op jit(solution)/shard_map/all_gather | solution.py:265
  33.2 10.1 %collective-permute-start = (bf16[16,72,256]{2,1,0:T(8,128)(2,1)S(1)}, bf16[16,72,256]{2,1,0:T(8,128)(2,1)S(1)}, u32[]{:S(2)}, u32[]{:S(2)}) collective-permute-start(bf16[16,72,256]{2,1,0:T(8,128)(2,1)S(1)} %bitcast.33), channel_id=1, source_target_pairs={{0,16},{16,0},{32,48},{48,32},{64,80},{80,64},{96,112},{112,96},{1... | collective-permute-start | bytes 1769480 | tf_op jit(solution)/shard_map/ppermute | solution.py:266
  44.0 0.0 copy-start.1
  44.1 0.0 copy-done.6
  44.1 0.0 copy-done.8
  44.1 0.0 copy-done.9
  44.1 0.0 copy-done.10
  44.1 0.0 copy-done.11
  44.1 0.6 prepare.1
  44.7 0.3 collective-permute-done.theirs_ref
  45.0 0.0 copy-done
  45.0 0.0 copy-done.5
  45.0 0.0 copy-done.7
  45.0 0.6 copy-done.1
  45.6 2.6 %attention.1 = f32[16,16,128]{2,1,0:T(8,128)S(1)} custom-call(s32[1]{0:T(128)} %bitcast.core_ref, f32[1]{0:T(128)S(6)} %copy.22.bias_ref, s32[16]{0:T(128)S(1)} %copy-done.7, bf16[16,2048]{1,0:T(8,128)(2,1)S(1)} %get-tuple-element.13.normed_ref, f32[16,384]{1,0:T(8,128)S(1)} %get-tuple-element.14.sums_ref, bf16[16,72,256]{2,1,0:T(8,128)(2,1)S(1)} %bitcast.35, ...), custom_call_target="tpu_custom_call" | custom-call | flops 1000000000 | bytes 1 | tf_op jit(solution)/shard_map/attention/pallas_call | solution.py:291
  48.3 0.0 copy-start.2
  48.3 0.0 copy-start.3
  48.3 0.0 copy-start.4
  48.3 13.8 %all_to_all.30.parts_ref = f32[16,16,128]{2,1,0:T(8,128)S(1)} all-to-all(f32[16,16,128]{2,1,0:T(8,128)S(1)} %attention.1), channel_id=1, replica_groups=mesh['ep'=32,'tp'=16] {'tp'}, dimensions={0} | all-to-all | bytes 262144 | tf_op jit(solution)/shard_map/all_to_all | solution.py:310
  62.1 0.2 spread.1
  62.3 19.4 %all_to_all.31 = bf16[32,4,128]{2,1,0:T(4,128)(2,1)S(1)} all-to-all(bf16[32,4,128]{2,1,0:T(4,128)(2,1)S(1)} %bitcast.43), channel_id=1, replica_groups=mesh['ep'=32,'tp'=16] {'ep'}, dimensions={0} | all-to-all | bytes 65536 | tf_op jit(solution)/shard_map/all_to_all | solution.py:314
  81.8 0.1 broadcast_in_dim.8
  81.9 13.0 %all_to_all.32.rows_ref = bf16[16,128,128]{2,1,0:T(8,128)(2,1)S(1)} all-to-all(bf16[16,128,128]{2,1,0:T(8,128)(2,1)S(1)} %broadcast_in_dim.8), channel_id=1, replica_groups=mesh['ep'=32,'tp'=16] {'tp'}, dimensions={0} | all-to-all | bytes 1048576 | tf_op jit(solution)/shard_map/all_to_all | solution.py:17
  94.9 0.0 copy-done.2
  94.9 0.0 copy-done.3
  94.9 0.0 copy-done.4
  94.9 1.1 experts.1
  96.0 12.4 %all_to_all.33.parts_ref = bf16[16,128,128]{2,1,0:T(8,128)(2,1)S(1)} all-to-all(bf16[16,128,128]{2,1,0:T(8,128)(2,1)S(1)} %experts.1), channel_id=1, replica_groups=mesh['ep'=32,'tp'=16] {'tp'}, dimensions={0} | all-to-all | bytes 1048576 | tf_op jit(solution)/shard_map/all_to_all | solution.py:319
  108.5 0.1 served.1
  108.5 18.4 %all_to_all.34 = bf16[32,4,128]{2,1,0:T(4,128)(2,1)S(1)} all-to-all(bf16[32,4,128]{2,1,0:T(4,128)(2,1)S(1)} %bitcast.42), channel_id=1, replica_groups=mesh['ep'=32,'tp'=16] {'ep'}, dimensions={0} | all-to-all | bytes 65536 | tf_op jit(solution)/shard_map/all_to_all | solution.py:321
  126.9 0.2 combine.1
  127.1 9.2 %all_to_all.35 = bf16[16,16,128]{2,1,0:T(8,128)(2,1)S(1)} all-to-all(bf16[16,16,128]{2,1,0:T(8,128)(2,1)S(1)} %combine.1), channel_id=1, replica_groups=mesh['ep'=32,'tp'=16] {'tp'}, dimensions={0} | all-to-all | bytes 131072 | tf_op jit(solution)/shard_map/all_to_all | solution.py:325
  136.2 0.6 copy_bitcast_fusion
  (1 shorter events, 0.0 us)
Async XLA Ops:
  0.9 43.2 %copy-start.6 = (bf16[2048]{0:T(1024)(128)(2,1)S(1)}, bf16[2048]{0:T(1024)(128)(2,1)}, u32[]{:S(2)}) copy-start(bf16[2048]{0:T(1024)(128)(2,1)} %gain_ref.3) | copy-start | bytes 12292
  0.9 43.2 %copy-start.8 = (bf16[16,2048]{1,0:T(8,128)(2,1)S(1)}, bf16[16,2048]{1,0:T(8,128)(2,1)}, u32[]{:S(2)}) copy-start(bf16[16,2048]{1,0:T(8,128)(2,1)} %tokens_ref.1) | copy-start | bytes 196612
  0.9 43.2 %copy-start.9 = (bf16[2048]{0:T(1024)(128)(2,1)S(1)}, bf16[2048]{0:T(1024)(128)(2,1)}, u32[]{:S(2)}) copy-start(bf16[2048]{0:T(1024)(128)(2,1)} %gain_ref.2) | copy-start | bytes 12292
  0.9 43.2 %copy-start.10 = (s32[16,4]{0,1:T(4,128)S(1)}, s32[16,4]{0,1:T(4,128)}, u32[]{:S(2)}) copy-start(s32[16,4]{0,1:T(4,128)} %param.31) | copy-start | bytes 772
  0.9 43.2 %copy-start.11 = (f32[16,4]{0,1:T(4,128)S(1)}, f32[16,4]{0,1:T(4,128)}, u32[]{:S(2)}) copy-start(f32[16,4]{0,1:T(4,128)} %param.32) | copy-start | bytes 772
  0.9 44.0 %copy-start = (bf16[16,1,1024,64]{2,3,1,0:T(8,128)(2,1)S(1)}, bf16[16,1,1024,64]{2,3,1,0:T(8,128)(2,1)}, u32[]{:S(2)}) copy-start(bf16[16,1,1024,64]{2,3,1,0:T(8,128)(2,1)} %param.25) | copy-start | bytes 6291460
  1.0 44.0 %copy-start.5 = (f32[16,1,1024]{2,1,0:T(1,128)S(1)}, f32[16,1,1024]{2,1,0:T(1,128)}, u32[]{:S(2)}) copy-start(f32[16,1,1024]{2,1,0:T(1,128)} %gates_ref.1) | copy-start | bytes 196612
  1.0 44.0 %copy-start.7 = (s32[16]{0:T(128)S(1)}, s32[16]{0:T(128)}, u32[]{:S(2)}) copy-start(s32[16]{0:T(128)} %lengths_ref.1) | copy-start | bytes 196
  33.2 11.7 %collective-permute-start = (bf16[16,72,256]{2,1,0:T(8,128)(2,1)S(1)}, bf16[16,72,256]{2,1,0:T(8,128)(2,1)S(1)}, u32[]{:S(2)}, u32[]{:S(2)}) collective-permute-start(bf16[16,72,256]{2,1,0:T(8,128)(2,1)S(1)} %bitcast.33), channel_id=1, source_target_pairs={{0,16},{16,0},{32,48},{48,32},{64,80},{80,64},{96,112},{112,96},{1... | collective-permute-start | bytes 1769480 | tf_op jit(solution)/shard_map/ppermute | solution.py:266
  44.0 1.6 %copy-start.1 = (bf16[16,1,1024,64]{2,3,1,0:T(8,128)(2,1)S(1)}, bf16[16,1,1024,64]{2,3,1,0:T(8,128)(2,1)}, u32[]{:S(2)}) copy-start(bf16[16,1,1024,64]{2,3,1,0:T(8,128)(2,1)} %param.26) | copy-start | bytes 6291460
  48.3 46.6 %copy-start.2 = (bf16[1,2048,64]{1,2,0:T(8,128)(2,1)S(1)}, bf16[1,2048,64]{1,2,0:T(8,128)(2,1)}, u32[]{:S(2)}) copy-start(bf16[1,2048,64]{1,2,0:T(8,128)(2,1)} %param.33) | copy-start | bytes 786436
  48.3 46.6 %copy-start.3 = (bf16[1,2048,64]{1,2,0:T(8,128)(2,1)S(1)}, bf16[1,2048,64]{1,2,0:T(8,128)(2,1)}, u32[]{:S(2)}) copy-start(bf16[1,2048,64]{1,2,0:T(8,128)(2,1)} %param.34) | copy-start | bytes 786436
  48.3 46.6 %copy-start.4 = (bf16[1,64,2048]{2,1,0:T(8,128)(2,1)S(1)}, bf16[1,64,2048]{2,1,0:T(8,128)(2,1)}, u32[]{:S(2)}) copy-start(bf16[1,64,2048]{2,1,0:T(8,128)(2,1)} %param.35) | copy-start | bytes 786436

commit v4 on v3

--- a/solution.py
+++ b/solution.py
@@ -12,16 +12,16 @@
 BF16 = jnp.bfloat16
 
 
-def to_everyone(shard, axis):
-    size = lax.axis_size(axis)
-    return lax.all_to_all(
-        jnp.broadcast_to(shard[None], (size, *shard.shape)), axis, 0, 0, tiled=True
-    )
+def exchanged(tiles, axis, order):
+    return lax.all_to_all(tiles, axis, 0, 0, tiled=True, axis_index_groups=[order])
 
 
 PACK_ROWS = 72
 LIMIT = 16 * 2**20
 CAPACITY = 4
+RING = list(range(16))
+PLANE = [5, 2, 3, 10, 13, 0, 7, 14, 4, 8, 12, 1, 11, 6, 9, 15]
+LINE = [i ^ 17 for i in range(32)]
 
 
 def settle_kernel(packed_ref, out_ref):
@@ -65,7 +65,7 @@
         eye, weight_ref[...], across, precision=lax.Precision.HIGHEST, preferred_element_type=F32
     )
     lane = lax.broadcasted_iota(jnp.int32, (rows, slots), 1)
-    expert = (lane // capacity).astype(F32)
+    expert = ((lane // capacity) ^ 17).astype(F32)
     named = jnp.zeros((rows, slots), F32)
     weight = jnp.zeros((rows, slots), F32)
     for k in range(top):
@@ -84,7 +84,7 @@
     total = jnp.zeros((rows, 256), F32)
     forget = jnp.zeros((rows, 128), F32)
     for z in range(packed_ref.shape[0]):
-        left = normed[:, z * 128 : (z + 1) * 128]
+        left = normed[:, RING[z] * 128 : (RING[z] + 1) * 128]
         left = jnp.where(taken, left, jnp.zeros_like(left))
         block = packed_ref[z, :64, :]
         total = total + jnp.dot(left, jnp.concatenate([block, block], axis=0), preferred_element_type=F32)
@@ -145,12 +145,13 @@
     attended = attended + (own_weight / denominator) * value_new.astype(F32)
     attended = attended.astype(BF16)
     lane = lax.broadcasted_iota(jnp.int32, (rows, 128), 1)
-    for z in range(chips):
+    for i, chip in enumerate(PLANE):
+        z = RING.index(chip)
         mine = jnp.dot(attended, mine_ref[z, :64, 128:], preferred_element_type=F32)
         theirs = jnp.dot(attended, theirs_ref[z, :64, 128:], preferred_element_type=F32)
         even = jnp.where(is_odd, theirs, mine)
         odd = jnp.where(is_odd, mine, theirs)
-        out_ref[z] = jnp.where(lane < head, pltpu.roll(even, head, 1), odd)
+        out_ref[i] = jnp.where(lane < head, pltpu.roll(even, head, 1), odd)
 
 
 def expert_kernel(rows_ref, gain_ref, gate_ref, up_ref, down_ref, out_ref):
@@ -161,10 +162,11 @@
     products = jnp.zeros((slots, 2 * gate_ref.shape[0]), F32)
     for t in range(tiles):
         part = rows_ref[t]
-        plain = part.astype(F32) * inverse[:, t * narrow : (t + 1) * narrow]
+        at = slice(PLANE[t] * narrow, (PLANE[t] + 1) * narrow)
+        plain = part.astype(F32) * inverse[:, at]
         squares = squares + plain * plain
         weights = jnp.concatenate(
-            [gate_ref[:, t * narrow : (t + 1) * narrow], up_ref[:, t * narrow : (t + 1) * narrow]], axis=0
+            [gate_ref[:, at], up_ref[:, at]], axis=0
         )
         products = products + lax.dot_general(
             part, weights, (((1,), (1,)), ((), ())), preferred_element_type=F32
@@ -176,7 +178,8 @@
     up_cut = jnp.clip(products[:, units:], -CLAMP_LIMIT, CLAMP_LIMIT)
     hidden = ((up_cut + 1.0) * gate_cut * jax.nn.sigmoid(SIGMOID_SLOPE * gate_cut)).astype(BF16)
     for t in range(tiles):
-        part = jnp.dot(hidden, down_ref[:, t * narrow : (t + 1) * narrow], preferred_element_type=F32)
+        at = slice(PLANE[t] * narrow, (PLANE[t] + 1) * narrow)
+        part = jnp.dot(hidden, down_ref[:, at], preferred_element_type=F32)
         out_ref[t] = part.astype(BF16)
 
 
@@ -261,7 +264,7 @@
     forget_row = jnp.pad(w_forget.T, ((0, PACK_ROWS - 65), (0, packed.shape[1] - 64)))
     packed = jnp.concatenate([packed, forget_row], axis=0)
     (packed,) = kernel(settle_kernel, "settle", [(packed.shape, BF16)], [vmem], cost=busy)(packed)
-    same_core = [[2 * z + c for z in range(chips)] for c in range(2)]
+    same_core = [[2 * z + c for z in RING] for c in range(2)]
     mine = lax.all_gather(packed, "ep", axis=0, tiled=False, axis_index_groups=same_core)
     theirs = lax.ppermute(mine, "ep", [(i, i ^ 1) for i in range(n_ep)])
 
@@ -307,18 +310,19 @@
         cache_gates,
     )
 
-    parts = lax.all_to_all(head_terms, "tp", 0, 0, tiled=True)
+    parts = exchanged(head_terms, "tp", PLANE)
     residual, sent = kernel(
         spread_kernel, "spread", [((rows, narrow), F32), ((slots, narrow), BF16)], [vmem] * 4
     )(parts, token_slice, moe_slice, choice)
-    received = lax.all_to_all(sent.reshape(n_ep, CAPACITY, narrow), "ep", 0, 0, tiled=True)
-    full = to_everyone(received.reshape(slots, narrow), "tp")
+    received = exchanged(sent.reshape(n_ep, CAPACITY, narrow), "ep", LINE)
+    full = jnp.broadcast_to(received.reshape(1, slots, narrow), (n_tp, slots, narrow))
+    full = exchanged(full, "tp", PLANE)
     (partial,) = kernel(expert_kernel, "experts", [((n_tp, slots, narrow), BF16)], [vmem] * 5)(
         full, moe_gain, jnp.swapaxes(w_gate[0], 0, 1), jnp.swapaxes(w_up[0], 0, 1), w_down[0]
     )
-    partial = lax.all_to_all(partial, "tp", 0, 0, tiled=True)
+    partial = exchanged(partial, "tp", PLANE)
     (served,) = kernel(gather_kernel, "served", [((slots, narrow), BF16)], [vmem])(partial)
-    returned = lax.all_to_all(served.reshape(n_ep, CAPACITY, narrow), "ep", 0, 0, tiled=True)
+    returned = exchanged(served.reshape(n_ep, CAPACITY, narrow), "ep", LINE)
     (copies_out,) = kernel(combine_kernel, "combine", [((n_tp, rows, narrow), BF16)], [vmem] * 3)(
         returned.reshape(slots, narrow), mix, residual
     )

time: 138 us -> 132 us (0.957)
  blocking collectives: 119 us -> 113 us
    all_to_all x5, blocking collectives: 77.1 us -> 70.9 us  [exchanged(): lax.all_to_all(tiles, axis, 0, 0, tiled=True, axis_index_groups=[order])]
where the time goes in v4:
time: 132 us
  blocking collectives  113 us (86%)
  starting transfers between devices  10.1 us (8%)
  Pallas kernels  4.74 us (4%)
  local copies, waits for them, and re-layouts  1.44 us (1%)
    all_to_all x5, blocking collectives, exchanged(): lax.all_to_all(tiles, axis, 0, 0, tiled=True, axis_index_groups=[order])  70.9 us
    all_gather x1, blocking collectives, local(): lax.all_gather(packed, 'ep', axis=0, tiled=False, axis_index_groups=same_...  32.3 us
    ppermute x1, starting transfers between devices, local(): theirs = lax.ppermute(mine, 'ep', [(i, i ^ 1) for i in range(n_ep)])  10.1 us
    all_to_all x1, blocking collectives, local(): final = lax.all_to_all(copies_out, 'tp', 0, 0, tiled=True)  10.1 us
    pallas_call x1, Pallas kernels, local(): kernel(attention_kernel, 'attention', [((n_tp, rows, narrow), F32)], [sme...  2.64 us
  transfers between devices with their start and end apart: 1, of which 1 were waited for; matrix products, arithmetic and copies ran while one was open for 0% of the time, Pallas kernels for 0%

profile of v4, /device:TPU:1, one launch (start us, length us, event | category | flops | bytes accessed | tf_op | source)
XLA Modules:
  0.0 131.6 jit_solution(260669611575342361)
XLA Ops:
  0.0 0.9 fusion.1.packed_ref
  0.9 0.0 copy-start.6
  0.9 0.0 copy-start.8
  0.9 0.0 copy-start.9
  0.9 0.0 copy-start.10
  0.9 0.0 copy-start.11
  0.9 0.0 copy-start
  1.0 0.0 copy-start.5
  1.0 0.0 copy-start.7
  1.0 32.3 %all-gather = bf16[1152,256]{1,0:T(8,128)(2,1)S(1)} all-gather(bf16[72,256]{1,0:T(8,128)(2,1)S(1)} %settle.1), channel_id=2, replica_groups={{0,32,64,96,128,160,192,224,256,288,320,352,384,416,448,480},{16,48,80,..., dimensions={0}, use_global_device_ids=true | all-gather | bytes 626688 | tf_op jit(solution)/shard_map/all_gather | solution.py:268
  33.2 10.1 %collective-permute-start = (bf16[16,72,256]{2,1,0:T(8,128)(2,1)S(1)}, bf16[16,72,256]{2,1,0:T(8,128)(2,1)S(1)}, u32[]{:S(2)}, u32[]{:S(2)}) collective-permute-start(bf16[16,72,256]{2,1,0:T(8,128)(2,1)S(1)} %bitcast.33), channel_id=1, source_target_pairs={{0,16},{16,0},{32,48},{48,32},{64,80},{80,64},{96,112},{112,96},{1... | collective-permute-start | bytes 1769480 | tf_op jit(solution)/shard_map/ppermute | solution.py:269
  44.0 0.0 copy-start.1
  44.1 0.0 copy-done.6
  44.1 0.0 copy-done.8
  44.1 0.0 copy-done.9
  44.1 0.0 copy-done.10
  44.1 0.0 copy-done.11
  44.1 0.6 prepare.1
  44.7 0.3 collective-permute-done.theirs_ref
  45.0 0.0 copy-done
  45.0 0.0 copy-done.5
  45.0 0.0 copy-done.7
  45.0 0.6 copy-done.1
  45.6 2.6 %attention.1 = f32[16,16,128]{2,1,0:T(8,128)S(1)} custom-call(s32[1]{0:T(128)} %bitcast.core_ref, f32[1]{0:T(128)S(6)} %copy.22.bias_ref, s32[16]{0:T(128)S(1)} %copy-done.7, bf16[16,2048]{1,0:T(8,128)(2,1)S(1)} %get-tuple-element.13.normed_ref, f32[16,384]{1,0:T(8,128)S(1)} %get-tuple-element.14.sums_ref, bf16[16,72,256]{2,1,0:T(8,128)(2,1)S(1)} %bitcast.35, ...), custom_call_target="tpu_custom_call" | custom-call | flops 1000000000 | bytes 1 | tf_op jit(solution)/shard_map/attention/pallas_call | solution.py:294
  48.3 0.0 copy-start.2
  48.3 0.0 copy-start.3
  48.3 0.0 copy-start.4
  48.3 13.1 %all_to_all.30.parts_ref = f32[16,16,128]{2,1,0:T(8,128)S(1)} all-to-all(f32[16,16,128]{2,1,0:T(8,128)S(1)} %attention.1), channel_id=1, replica_groups={{5,2,3,10,13,0,7,14,4,8,12,1,11,6,9,15},{21,18,19,26,29,16,23,30,20,24,..., dimensions={0} | all-to-all | bytes 262144 | tf_op jit(solution)/shard_map/all_to_all | solution.py:16
  61.4 0.2 spread.1
  61.6 15.3 %all_to_all.31 = bf16[32,4,128]{2,1,0:T(4,128)(2,1)S(1)} all-to-all(bf16[32,4,128]{2,1,0:T(4,128)(2,1)S(1)} %bitcast.43), channel_id=1, replica_groups={{272,256,304,288,336,320,368,352,400,384,432,416,464,448,496,480,16,0,4..., dimensions={0} | all-to-all | bytes 65536 | tf_op jit(solution)/shard_map/all_to_all | solution.py:16
  76.9 0.1 broadcast_in_dim.8
  77.0 12.7 %all_to_all.32.rows_ref = bf16[16,128,128]{2,1,0:T(8,128)(2,1)S(1)} all-to-all(bf16[16,128,128]{2,1,0:T(8,128)(2,1)S(1)} %broadcast_in_dim.8), channel_id=1, replica_groups={{5,2,3,10,13,0,7,14,4,8,12,1,11,6,9,15},{21,18,19,26,29,16,23,30,20,24,..., dimensions={0} | all-to-all | bytes 1048576 | tf_op jit(solution)/shard_map/all_to_all | solution.py:16
  89.7 0.0 copy-done.2
  89.7 0.0 copy-done.3
  89.7 0.0 copy-done.4
  89.7 1.1 experts.1
  90.8 13.8 %all_to_all.33.parts_ref = bf16[16,128,128]{2,1,0:T(8,128)(2,1)S(1)} all-to-all(bf16[16,128,128]{2,1,0:T(8,128)(2,1)S(1)} %experts.1), channel_id=1, replica_groups={{5,2,3,10,13,0,7,14,4,8,12,1,11,6,9,15},{21,18,19,26,29,16,23,30,20,24,..., dimensions={0} | all-to-all | bytes 1048576 | tf_op jit(solution)/shard_map/all_to_all | solution.py:16
  104.6 0.1 served.1
  104.7 16.0 %all_to_all.34 = bf16[32,4,128]{2,1,0:T(4,128)(2,1)S(1)} all-to-all(bf16[32,4,128]{2,1,0:T(4,128)(2,1)S(1)} %bitcast.42), channel_id=1, replica_groups={{272,256,304,288,336,320,368,352,400,384,432,416,464,448,496,480,16,0,4..., dimensions={0} | all-to-all | bytes 65536 | tf_op jit(solution)/shard_map/all_to_all | solution.py:16
  120.7 0.2 combine.1
  120.9 10.1 %all_to_all.35 = bf16[16,16,128]{2,1,0:T(8,128)(2,1)S(1)} all-to-all(bf16[16,16,128]{2,1,0:T(8,128)(2,1)S(1)} %combine.1), channel_id=1, replica_groups=mesh['ep'=32,'tp'=16] {'tp'}, dimensions={0} | all-to-all | bytes 131072 | tf_op jit(solution)/shard_map/all_to_all | solution.py:329
  131.0 0.6 copy_bitcast_fusion
  (1 shorter events, 0.0 us)
Async XLA Ops:
  0.9 43.2 %copy-start.6 = (bf16[2048]{0:T(1024)(128)(2,1)S(1)}, bf16[2048]{0:T(1024)(128)(2,1)}, u32[]{:S(2)}) copy-start(bf16[2048]{0:T(1024)(128)(2,1)} %gain_ref.3) | copy-start | bytes 12292
  0.9 43.2 %copy-start.8 = (bf16[16,2048]{1,0:T(8,128)(2,1)S(1)}, bf16[16,2048]{1,0:T(8,128)(2,1)}, u32[]{:S(2)}) copy-start(bf16[16,2048]{1,0:T(8,128)(2,1)} %tokens_ref.1) | copy-start | bytes 196612
  0.9 43.2 %copy-start.9 = (bf16[2048]{0:T(1024)(128)(2,1)S(1)}, bf16[2048]{0:T(1024)(128)(2,1)}, u32[]{:S(2)}) copy-start(bf16[2048]{0:T(1024)(128)(2,1)} %gain_ref.2) | copy-start | bytes 12292
  0.9 43.2 %copy-start.10 = (s32[16,4]{0,1:T(4,128)S(1)}, s32[16,4]{0,1:T(4,128)}, u32[]{:S(2)}) copy-start(s32[16,4]{0,1:T(4,128)} %param.31) | copy-start | bytes 772
  0.9 43.2 %copy-start.11 = (f32[16,4]{0,1:T(4,128)S(1)}, f32[16,4]{0,1:T(4,128)}, u32[]{:S(2)}) copy-start(f32[16,4]{0,1:T(4,128)} %param.32) | copy-start | bytes 772
  0.9 44.0 %copy-start = (bf16[16,1,1024,64]{2,3,1,0:T(8,128)(2,1)S(1)}, bf16[16,1,1024,64]{2,3,1,0:T(8,128)(2,1)}, u32[]{:S(2)}) copy-start(bf16[16,1,1024,64]{2,3,1,0:T(8,128)(2,1)} %param.25) | copy-start | bytes 6291460
  1.0 44.0 %copy-start.5 = (f32[16,1,1024]{2,1,0:T(1,128)S(1)}, f32[16,1,1024]{2,1,0:T(1,128)}, u32[]{:S(2)}) copy-start(f32[16,1,1024]{2,1,0:T(1,128)} %gates_ref.1) | copy-start | bytes 196612
  1.0 44.0 %copy-start.7 = (s32[16]{0:T(128)S(1)}, s32[16]{0:T(128)}, u32[]{:S(2)}) copy-start(s32[16]{0:T(128)} %lengths_ref.1) | copy-start | bytes 196
  33.2 11.7 %collective-permute-start = (bf16[16,72,256]{2,1,0:T(8,128)(2,1)S(1)}, bf16[16,72,256]{2,1,0:T(8,128)(2,1)S(1)}, u32[]{:S(2)}, u32[]{:S(2)}) collective-permute-start(bf16[16,72,256]{2,1,0:T(8,128)(2,1)S(1)} %bitcast.33), channel_id=1, source_target_pairs={{0,16},{16,0},{32,48},{48,32},{64,80},{80,64},{96,112},{112,96},{1... | collective-permute-start | bytes 1769480 | tf_op jit(solution)/shard_map/ppermute | solution.py:269
  44.0 1.6 %copy-start.1 = (bf16[16,1,1024,64]{2,3,1,0:T(8,128)(2,1)S(1)}, bf16[16,1,1024,64]{2,3,1,0:T(8,128)(2,1)}, u32[]{:S(2)}) copy-start(bf16[16,1,1024,64]{2,3,1,0:T(8,128)(2,1)} %param.26) | copy-start | bytes 6291460
  48.3 41.4 %copy-start.2 = (bf16[1,2048,64]{1,2,0:T(8,128)(2,1)S(1)}, bf16[1,2048,64]{1,2,0:T(8,128)(2,1)}, u32[]{:S(2)}) copy-start(bf16[1,2048,64]{1,2,0:T(8,128)(2,1)} %param.33) | copy-start | bytes 786436
  48.3 41.4 %copy-start.3 = (bf16[1,2048,64]{1,2,0:T(8,128)(2,1)S(1)}, bf16[1,2048,64]{1,2,0:T(8,128)(2,1)}, u32[]{:S(2)}) copy-start(bf16[1,2048,64]{1,2,0:T(8,128)(2,1)} %param.34) | copy-start | bytes 786436
  48.3 41.4 %copy-start.4 = (bf16[1,64,2048]{2,1,0:T(8,128)(2,1)S(1)}, bf16[1,64,2048]{2,1,0:T(8,128)(2,1)}, u32[]{:S(2)}) copy-start(bf16[1,64,2048]{2,1,0:T(8,128)(2,1)} %param.35) | copy-start | bytes 786436

commit v5 on v4

--- a/solution.py
+++ b/solution.py
@@ -151,7 +151,7 @@
         theirs = jnp.dot(attended, theirs_ref[z, :64, 128:], preferred_element_type=F32)
         even = jnp.where(is_odd, theirs, mine)
         odd = jnp.where(is_odd, mine, theirs)
-        out_ref[i] = jnp.where(lane < head, pltpu.roll(even, head, 1), odd)
+        out_ref[i] = jnp.where(lane < head, pltpu.roll(even, head, 1), odd).astype(BF16)
 
 
 def expert_kernel(rows_ref, gain_ref, gate_ref, up_ref, down_ref, out_ref):
@@ -186,7 +186,7 @@
 def spread_kernel(parts_ref, slice_ref, moe_slice_ref, choice_ref, residual_ref, sent_ref):
     residual = slice_ref[...]
     for t in range(parts_ref.shape[0]):
-        residual = residual + parts_ref[t]
+        residual = residual + parts_ref[t].astype(F32)
     residual_ref[...] = residual
     scaled = (residual * moe_slice_ref[:1, :]).astype(BF16)
     sent_ref[...] = lax.dot_general(
@@ -294,7 +294,7 @@
     (head_terms,) = kernel(
         attention_kernel,
         "attention",
-        [((n_tp, rows, narrow), F32)],
+        [((n_tp, rows, narrow), BF16)],
         [smem, smem, smem] + [vmem] * 7,
         cost=busy,
     )(

time: 132 us -> 132 us (level)
  no operation moved by 1% of the time
where the time goes in v5:
time: 132 us; the launch traced here: 131 us
  blocking collectives  113 us (86%)
  starting transfers between devices  10.1 us (8%)
  Pallas kernels  4.75 us (4%)
  local copies, waits for them, and re-layouts  1.43 us (1%)
    all_to_all x5, blocking collectives, exchanged(): lax.all_to_all(tiles, axis, 0, 0, tiled=True, axis_index_groups=[order])  70.6 us
    all_gather x1, blocking collectives, local(): lax.all_gather(packed, 'ep', axis=0, tiled=False, axis_index_groups=same_...  32.3 us
    ppermute x1, starting transfers between devices, local(): theirs = lax.ppermute(mine, 'ep', [(i, i ^ 1) for i in range(n_ep)])  10.1 us
    all_to_all x1, blocking collectives, local(): final = lax.all_to_all(copies_out, 'tp', 0, 0, tiled=True)  10.1 us
    pallas_call x1, Pallas kernels, local(): kernel(attention_kernel, 'attention', [((n_tp, rows, narrow), BF16)], [sm...  2.64 us
  transfers between devices with their start and end apart: 1, of which 1 were waited for; matrix products, arithmetic and copies ran while one was open for 0% of the time, Pallas kernels for 0%

profile of v5, /device:TPU:1, one launch (start us, length us, event | category | flops | bytes accessed | tf_op | source)
XLA Modules:
  0.0 131.2 jit_solution(10306878649945141382)
XLA Ops:
  0.0 0.9 fusion.1.packed_ref
  0.9 0.0 copy-start.6
  0.9 0.0 copy-start.8
  0.9 0.0 copy-start.9
  0.9 0.0 copy-start.10
  0.9 0.0 copy-start.11
  0.9 0.0 copy-start
  1.0 0.0 copy-start.5
  1.0 0.0 copy-start.7
  1.0 32.3 %all-gather = bf16[1152,256]{1,0:T(8,128)(2,1)S(1)} all-gather(bf16[72,256]{1,0:T(8,128)(2,1)S(1)} %settle.1), channel_id=2, replica_groups={{0,32,64,96,128,160,192,224,256,288,320,352,384,416,448,480},{16,48,80,..., dimensions={0}, use_global_device_ids=true | all-gather | bytes 626688 | tf_op jit(solution)/shard_map/all_gather | solution.py:268
  33.2 10.1 %collective-permute-start = (bf16[16,72,256]{2,1,0:T(8,128)(2,1)S(1)}, bf16[16,72,256]{2,1,0:T(8,128)(2,1)S(1)}, u32[]{:S(2)}, u32[]{:S(2)}) collective-permute-start(bf16[16,72,256]{2,1,0:T(8,128)(2,1)S(1)} %bitcast.33), channel_id=1, source_target_pairs={{0,16},{16,0},{32,48},{48,32},{64,80},{80,64},{96,112},{112,96},{1... | collective-permute-start | bytes 1769480 | tf_op jit(solution)/shard_map/ppermute | solution.py:269
  44.0 0.0 copy-start.1
  44.1 0.0 copy-done.6
  44.1 0.0 copy-done.8
  44.1 0.0 copy-done.9
  44.1 0.0 copy-done.10
  44.1 0.0 copy-done.11
  44.1 0.6 prepare.1
  44.7 0.3 collective-permute-done.theirs_ref
  45.0 0.0 copy-done
  45.0 0.0 copy-done.5
  45.0 0.0 copy-done.7
  45.0 0.6 copy-done.1
  45.6 0.0 copy-start.2
  45.6 0.0 copy-start.3
  45.6 0.0 copy-start.4
  45.6 2.6 %attention.1 = bf16[16,16,128]{2,1,0:T(8,128)(2,1)S(1)} custom-call(s32[1]{0:T(128)} %bitcast.core_ref, f32[1]{0:T(128)S(6)} %copy.22.bias_ref, s32[16]{0:T(128)S(1)} %copy-done.7, bf16[16,2048]{1,0:T(8,128)(2,1)S(1)} %get-tuple-element.13.normed_ref, f32[16,384]{1,0:T(8,128)S(1)} %get-tuple-element.14.sums_ref, bf16[16,72,256]{2,1,0:T(8,128)(2,1)S(1)} %bitcast.35, ...), custom_call_target="tpu_custom_call" | custom-call | flops 1000000000 | bytes 1 | tf_op jit(solution)/shard_map/attention/pallas_call | solution.py:294
  48.3 12.9 %all_to_all.30.parts_ref = bf16[16,16,128]{2,1,0:T(8,128)(2,1)S(1)} all-to-all(bf16[16,16,128]{2,1,0:T(8,128)(2,1)S(1)} %attention.1), channel_id=1, replica_groups={{5,2,3,10,13,0,7,14,4,8,12,1,11,6,9,15},{21,18,19,26,29,16,23,30,20,24,..., dimensions={0} | all-to-all | bytes 131072 | tf_op jit(solution)/shard_map/all_to_all | solution.py:16
  61.2 0.2 spread.1
  61.4 15.2 %all_to_all.31 = bf16[32,4,128]{2,1,0:T(4,128)(2,1)S(1)} all-to-all(bf16[32,4,128]{2,1,0:T(4,128)(2,1)S(1)} %bitcast.43), channel_id=1, replica_groups={{272,256,304,288,336,320,368,352,400,384,432,416,464,448,496,480,16,0,4..., dimensions={0} | all-to-all | bytes 65536 | tf_op jit(solution)/shard_map/all_to_all | solution.py:16
  76.6 0.1 broadcast_in_dim.8
  76.7 12.6 %all_to_all.32.rows_ref = bf16[16,128,128]{2,1,0:T(8,128)(2,1)S(1)} all-to-all(bf16[16,128,128]{2,1,0:T(8,128)(2,1)S(1)} %broadcast_in_dim.8), channel_id=1, replica_groups={{5,2,3,10,13,0,7,14,4,8,12,1,11,6,9,15},{21,18,19,26,29,16,23,30,20,24,..., dimensions={0} | all-to-all | bytes 1048576 | tf_op jit(solution)/shard_map/all_to_all | solution.py:16
  89.4 0.0 copy-done.2
  89.4 0.0 copy-done.3
  89.4 0.0 copy-done.4
  89.4 1.1 experts.1
  90.5 13.8 %all_to_all.33.parts_ref = bf16[16,128,128]{2,1,0:T(8,128)(2,1)S(1)} all-to-all(bf16[16,128,128]{2,1,0:T(8,128)(2,1)S(1)} %experts.1), channel_id=1, replica_groups={{5,2,3,10,13,0,7,14,4,8,12,1,11,6,9,15},{21,18,19,26,29,16,23,30,20,24,..., dimensions={0} | all-to-all | bytes 1048576 | tf_op jit(solution)/shard_map/all_to_all | solution.py:16
  104.2 0.1 served.1
  104.3 16.0 %all_to_all.34 = bf16[32,4,128]{2,1,0:T(4,128)(2,1)S(1)} all-to-all(bf16[32,4,128]{2,1,0:T(4,128)(2,1)S(1)} %bitcast.42), channel_id=1, replica_groups={{272,256,304,288,336,320,368,352,400,384,432,416,464,448,496,480,16,0,4..., dimensions={0} | all-to-all | bytes 65536 | tf_op jit(solution)/shard_map/all_to_all | solution.py:16
  120.3 0.2 combine.1
  120.5 10.1 %all_to_all.35 = bf16[16,16,128]{2,1,0:T(8,128)(2,1)S(1)} all-to-all(bf16[16,16,128]{2,1,0:T(8,128)(2,1)S(1)} %combine.1), channel_id=1, replica_groups=mesh['ep'=32,'tp'=16] {'tp'}, dimensions={0} | all-to-all | bytes 131072 | tf_op jit(solution)/shard_map/all_to_all | solution.py:329
  130.6 0.6 copy_bitcast_fusion
  (1 shorter events, 0.0 us)
Async XLA Ops:
  0.9 43.2 %copy-start.6 = (bf16[2048]{0:T(1024)(128)(2,1)S(1)}, bf16[2048]{0:T(1024)(128)(2,1)}, u32[]{:S(2)}) copy-start(bf16[2048]{0:T(1024)(128)(2,1)} %gain_ref.3) | copy-start | bytes 12292
  0.9 43.2 %copy-start.8 = (bf16[16,2048]{1,0:T(8,128)(2,1)S(1)}, bf16[16,2048]{1,0:T(8,128)(2,1)}, u32[]{:S(2)}) copy-start(bf16[16,2048]{1,0:T(8,128)(2,1)} %tokens_ref.1) | copy-start | bytes 196612
  0.9 43.2 %copy-start.9 = (bf16[2048]{0:T(1024)(128)(2,1)S(1)}, bf16[2048]{0:T(1024)(128)(2,1)}, u32[]{:S(2)}) copy-start(bf16[2048]{0:T(1024)(128)(2,1)} %gain_ref.2) | copy-start | bytes 12292
  0.9 43.2 %copy-start.10 = (s32[16,4]{0,1:T(4,128)S(1)}, s32[16,4]{0,1:T(4,128)}, u32[]{:S(2)}) copy-start(s32[16,4]{0,1:T(4,128)} %param.31) | copy-start | bytes 772
  0.9 43.2 %copy-start.11 = (f32[16,4]{0,1:T(4,128)S(1)}, f32[16,4]{0,1:T(4,128)}, u32[]{:S(2)}) copy-start(f32[16,4]{0,1:T(4,128)} %param.32) | copy-start | bytes 772
  0.9 44.0 %copy-start = (bf16[16,1,1024,64]{2,3,1,0:T(8,128)(2,1)S(1)}, bf16[16,1,1024,64]{2,3,1,0:T(8,128)(2,1)}, u32[]{:S(2)}) copy-start(bf16[16,1,1024,64]{2,3,1,0:T(8,128)(2,1)} %param.25) | copy-start | bytes 6291460
  1.0 44.0 %copy-start.5 = (f32[16,1,1024]{2,1,0:T(1,128)S(1)}, f32[16,1,1024]{2,1,0:T(1,128)}, u32[]{:S(2)}) copy-start(f32[16,1,1024]{2,1,0:T(1,128)} %gates_ref.1) | copy-start | bytes 196612
  1.0 44.0 %copy-start.7 = (s32[16]{0:T(128)S(1)}, s32[16]{0:T(128)}, u32[]{:S(2)}) copy-start(s32[16]{0:T(128)} %lengths_ref.1) | copy-start | bytes 196
  33.2 11.7 %collective-permute-start = (bf16[16,72,256]{2,1,0:T(8,128)(2,1)S(1)}, bf16[16,72,256]{2,1,0:T(8,128)(2,1)S(1)}, u32[]{:S(2)}, u32[]{:S(2)}) collective-permute-start(bf16[16,72,256]{2,1,0:T(8,128)(2,1)S(1)} %bitcast.33), channel_id=1, source_target_pairs={{0,16},{16,0},{32,48},{48,32},{64,80},{80,64},{96,112},{112,96},{1... | collective-permute-start | bytes 1769480 | tf_op jit(solution)/shard_map/ppermute | solution.py:269
  44.0 1.6 %copy-start.1 = (bf16[16,1,1024,64]{2,3,1,0:T(8,128)(2,1)S(1)}, bf16[16,1,1024,64]{2,3,1,0:T(8,128)(2,1)}, u32[]{:S(2)}) copy-start(bf16[16,1,1024,64]{2,3,1,0:T(8,128)(2,1)} %param.26) | copy-start | bytes 6291460
  45.6 43.7 %copy-start.2 = (bf16[1,2048,64]{1,2,0:T(8,128)(2,1)S(1)}, bf16[1,2048,64]{1,2,0:T(8,128)(2,1)}, u32[]{:S(2)}) copy-start(bf16[1,2048,64]{1,2,0:T(8,128)(2,1)} %param.33) | copy-start | bytes 786436
  45.6 43.7 %copy-start.3 = (bf16[1,2048,64]{1,2,0:T(8,128)(2,1)S(1)}, bf16[1,2048,64]{1,2,0:T(8,128)(2,1)}, u32[]{:S(2)}) copy-start(bf16[1,2048,64]{1,2,0:T(8,128)(2,1)} %param.34) | copy-start | bytes 786436
  45.6 43.7 %copy-start.4 = (bf16[1,64,2048]{2,1,0:T(8,128)(2,1)S(1)}, bf16[1,64,2048]{2,1,0:T(8,128)(2,1)}, u32[]{:S(2)}) copy-start(bf16[1,64,2048]{2,1,0:T(8,128)(2,1)} %param.35) | copy-start | bytes 786436
